TPU v7x, 32 devices: a whole 2x2x4 slice. The times are simulated.
32 devices in a mesh: kv: 8 (over z, x), tp: 4 (over y, core).
Axes of the slice: x: 2, y: 2, z: 4, core: 2. Of those that a mesh axis runs over, the one named last changes fastest.
Arguments:
- tokens: bfloat16 [256, 4096], P('kv', 'tp'), may hold values from -12 to 12
- norm_gain: float32 [4096], replicated, may hold values from 0.1 to 1.9
- query_weight: bfloat16 [4096, 4096], P('kv', 'tp'), may hold values from -0.09375 to 0.09375
- key_weight: bfloat16 [4096, 4096], P('kv', 'tp'), may hold values from -0.09375 to 0.09375
- value_weight: bfloat16 [4096, 4096], P('kv', 'tp'), may hold values from -0.09375 to 0.09375
- outgate_weight: bfloat16 [4096, 4096], P('kv', 'tp'), may hold values from -0.09375 to 0.09375
- ingate_weight: bfloat16 [4096, 16], replicated, may hold values from -0.09375 to 0.09375
- forget_weight: bfloat16 [4096, 16], replicated, may hold values from -0.09375 to 0.09375
- forget_bias: float32 [16], replicated, may hold values from 0.5 to 4
- output_weight: bfloat16 [4096, 4096], P('tp', 'kv'), may hold values from -0.09375 to 0.09375
- state_memory: float32 [64, 16, 256, 256], P('kv', 'tp'), may hold values from -0.8 to 0.8
- state_normaliser: float32 [64, 16, 256], P('kv', 'tp'), may hold values from -0.8 to 0.8
- state_stabiliser: float32 [64, 16], P('kv', 'tp'), may hold values from -4 to 4
- past_keys: bfloat16 [64, 4, 4096], P('kv', None, 'tp'), may hold values from -6 to 6
- past_values: bfloat16 [64, 4, 4096], P('kv', None, 'tp'), may hold values from -6 to 6
- past_ingate: float32 [64, 4, 16], P('kv', None, 'tp'), may hold values from -4 to 4
- past_forget: float32 [64, 4, 16], P('kv', None, 'tp'), may hold values from -1 to 4
- accepted: int32 [64], P('kv'), may hold values from 0 to 4
Outputs:
- mixed: bfloat16 [256, 4096], P('kv', 'tp')
- taken_memory: float32 [64, 16, 256, 256], P('kv', 'tp')
- taken_normaliser: float32 [64, 16, 256], P('kv', 'tp')
- taken_stabiliser: float32 [64, 16], P('kv', 'tp')
- new_keys: bfloat16 [256, 4096], P('kv', 'tp')
- new_values: bfloat16 [256, 4096], P('kv', 'tp')
All inputs are finite; a program needn't handle non-finite values.
Results may differ from a plain program's by a relative error of at most 0.03.
Values may be sent and summed in bfloat16 or wider, within the bound.
A program may use at most 64 MiB of HBM per device.

v0:
```python
import functools

import jax
import jax.numpy as jnp
from jax import lax
from jax.experimental import pallas as pl
from jax.experimental.pallas import tpu as pltpu
from jax.sharding import PartitionSpec as P

epsilon = 1e-06
MESH = pl.DeviceIdType.MESH
vmem = pl.BlockSpec(memory_space=pltpu.VMEM)


def heads_view(rows, seq_count, head_count):
    shaped = rows.astype(jnp.float32).reshape(
        seq_count, -1, head_count, rows.shape[-1] // head_count
    )
    return shaped.transpose(0, 2, 1, 3)


def catch_up(normaliser, stabiliser, key_rows, in_gate, forget_pre, taken_mask):
    log_forget = jnp.where(taken_mask, jax.nn.log_sigmoid(forget_pre), 0.0)
    running = jnp.cumsum(log_forget, axis=-1)
    chain_total = running[..., -1]
    end_logs = jnp.where(taken_mask, chain_total[..., None] - running + in_gate, -jnp.inf)
    stable_new = jnp.maximum(chain_total + stabiliser, jnp.max(end_logs, axis=-1))
    carry_decay = jnp.exp(chain_total + stabiliser - stable_new)
    weighted = key_rows * jnp.exp(end_logs - stable_new[..., None])[..., None]
    normaliser_new = carry_decay[..., None] * normaliser + jnp.sum(weighted, axis=-2)
    return (carry_decay, weighted, normaliser_new, stable_new)


def advance(from_memory, normaliser, stabiliser, query_rows, key_rows, values, in_gate, forget_pre):
    chain_len = query_rows.shape[-2]
    running = jnp.cumsum(jax.nn.log_sigmoid(forget_pre), axis=-1)
    causal = jnp.arange(chain_len)[:, None] >= jnp.arange(chain_len)[None, :]
    within = jnp.where(
        causal, running[..., :, None] - running[..., None, :] + in_gate[..., None, :], -jnp.inf
    )
    carried = running + stabiliser[..., None]
    stable = jnp.maximum(carried, jnp.max(within, axis=-1))
    scores = jnp.einsum("...td,...sd->...ts", query_rows, key_rows) * jnp.exp(
        within - stable[..., None]
    )
    carry_weight = jnp.exp(carried - stable)
    numerator = carry_weight[..., None] * from_memory
    numerator = numerator + jnp.einsum("...ts,...se->...te", scores, values)
    denominator = carry_weight * jnp.sum(query_rows * normaliser[..., None, :], axis=-1) + jnp.sum(
        scores, axis=-1
    )
    return numerator / jnp.maximum(jnp.abs(denominator), 1.0)[..., None]


def signal(sem, kv, tp):
    pl.semaphore_signal(sem, inc=1, device_id={"kv": kv, "tp": tp}, device_id_type=MESH)


def remote(src, dst, send_sem, recv_sem, kv, tp):
    return pltpu.make_async_remote_copy(
        src_ref=src,
        dst_ref=dst,
        send_sem=send_sem,
        recv_sem=recv_sem,
        device_id={"kv": kv, "tp": tp},
        device_id_type=MESH,
    )


def each(count, step, start=0):
    def run(index, carry):
        step(index)
        return carry

    lax.fori_loop(start, count, run, 0)


def project_kernel(
    n, m, squares_at, features,
    tok, gain, gate_part, w0, w1, w2, w3, decay, past_k, past_v, memory,
    o0, o1, o2, o3, gates, from_memory, memory_out,
    x_buf, s_buf, near, pair, far, g_buf, m_buf, m_low,
    x_send, x_recv, s_send, s_recv, f_send, f_recv, g_send, g_recv, m_in, m_out,
):
    k = lax.axis_index("kv")
    t = lax.axis_index("tp")
    r = n // m
    width = x_buf.shape[2]
    rows = x_buf.shape[1]
    half = n // 2
    z = k // 2
    x = k % 2
    seqs, heads, dk, dv = m_buf.shape
    t0 = k // r
    mine = k % r
    to_self = t0 == t

    def load(q):
        return pltpu.make_async_copy(memory.at[q], m_buf.at[q], m_in.at[q])

    def store(q):
        return pltpu.make_async_copy(m_buf.at[q], memory_out.at[q], m_out.at[q])

    each(seqs, lambda q: load(q).start())
    barrier = pltpu.get_barrier_semaphore()

    def greet_source(i):
        kk = lax.rem(k + i, n)

        @pl.when(jnp.logical_not(jnp.logical_and(i == 0, to_self)))
        def _():
            signal(barrier, kk, t0)

    each(n, greet_source)
    each(n, lambda i: signal(barrier, lax.rem(k + i, n), t), 1)
    each(m, lambda j: signal(barrier, k, lax.rem(t + j, m)), 1)
    pl.semaphore_wait(barrier, n + (n - 1) + (m - 1) - to_self.astype(jnp.int32))

    def token_copy(q):
        h = q // m
        tt = lax.rem(q + t, m)
        kk = t * r + h
        same = jnp.logical_and(kk == k, tt == t)
        cols = pl.ds(pl.multiple_of(h * width, width), width)
        return same, remote(
            tok.at[:, cols], x_buf.at[k], x_send.at[q], x_recv.at[k], kk, tt
        )

    def start_tokens(q):
        same, copy = token_copy(q)

        @pl.when(jnp.logical_not(same))
        def _():
            copy.start()

    each(n, start_tokens)

    def gate_copy(j):
        return remote(
            gate_part, g_buf.at[j - 1], g_send.at[j - 1], g_recv.at[j - 1], k, lax.rem(t + j, m)
        )

    each(m, lambda j: gate_copy(j).start(), 1)

    @pl.when(to_self)
    def _():
        cols = pl.ds(pl.multiple_of(mine * width, width), width)
        x_buf[k] = tok[:, cols]

    def wait_tokens(kk):
        @pl.when(jnp.logical_not(jnp.logical_and(kk == k, to_self)))
        def _():
            remote(
                tok.at[:, pl.ds(0, width)], x_buf.at[kk], x_send.at[0], x_recv.at[kk], k, t
            ).wait_recv()

    each(n, wait_tokens)
    own_gain = gain[:, pl.ds(pl.multiple_of(k * width, width), width)]
    scaled = (x_buf[...].reshape(n * rows, width).astype(jnp.float32) * own_gain).astype(
        jnp.bfloat16
    )

    def near_copy(c, i):
        return remote(
            s_buf.at[c, i * 2 + 1 - x],
            near.at[c, i],
            s_send.at[c, i],
            s_recv.at[c, i],
            z * 2 + 1 - x,
            t,
        )

    def far_copy(c, i):
        to = lax.rem(z + i, half)
        return remote(
            pair.at[c, to], far.at[c, i - 1], f_send.at[c, i - 1], f_recv.at[c, i - 1], to * 2 + x, t
        )

    for c, w in enumerate((w0, w1, w2, w3)):
        part = jnp.dot(scaled, w[...], preferred_element_type=jnp.float32)
        s_buf[c] = part.astype(jnp.bfloat16).reshape(n, rows, -1)
        each(half, lambda i, c=c: near_copy(c, i).start())

    def take(q):
        load(q).wait()
        for h in range(heads):
            added = lax.dot_general(
                past_k[q, :, h * dk : (h + 1) * dk],
                past_v[q, :, h * dv : (h + 1) * dv],
                (((0,), (0,)), ((), ())),
                preferred_element_type=jnp.float32,
            )
            new = decay[q * heads + h] * m_buf[q, h] + added
            m_buf[q, h] = new
            m_low[q, h] = new.astype(jnp.bfloat16)
        store(q).start()

    for c in range(4):
        each(seqs * (c + 1) // 4, take, seqs * c // 4)
        each(half, lambda i, c=c: near_copy(c, i).wait_recv())

        def fold(i, c=c):
            pair[c, i] = (
                s_buf[c, i * 2 + x].astype(jnp.float32) + near[c, i].astype(jnp.float32)
            ).astype(jnp.bfloat16)

        each(half, fold)
        each(half, lambda i, c=c: far_copy(c, i).start(), 1)

    each(m, lambda j: gate_copy(j).wait_recv(), 1)
    total = gate_part[...]
    for j in range(m - 1):
        total = total + g_buf[j]
    scale = lax.rsqrt(total[:, squares_at : squares_at + 1] / features + epsilon)
    gates[...] = total * scale
    for c, out in enumerate((o0, o1, o2, o3)):
        each(half, lambda i, c=c: far_copy(c, i).wait_recv(), 1)
        summed = pair[c, z].astype(jnp.float32)
        for i in range(half - 1):
            summed = summed + far[c, i].astype(jnp.float32)
        out[...] = (summed * scale).astype(jnp.bfloat16)
        if c == 0:
            chain = rows // seqs
            row_seq = lax.broadcasted_iota(jnp.int32, (rows, dv), 0) // chain
            for h in range(heads):
                query = o0[:, h * dk : (h + 1) * dk]
                acc = jnp.zeros((rows, dv), jnp.float32)
                for q in range(seqs):
                    got = jnp.dot(query, m_low[q, h], preferred_element_type=jnp.float32)
                    acc = jnp.where(row_seq == q, got, acc)
                from_memory[:, h * dv : (h + 1) * dv] = acc

    def drain_tokens(q):
        same, copy = token_copy(q)

        @pl.when(jnp.logical_not(same))
        def _():
            copy.wait_send()

    each(n, drain_tokens)
    each(m, lambda j: gate_copy(j).wait_send(), 1)
    for c in range(4):
        each(half, lambda i, c=c: near_copy(c, i).wait_send())
        each(half, lambda i, c=c: far_copy(c, i).wait_send(), 1)
    each(seqs, lambda q: store(q).wait())


def project(n, m, squares_at, tokens, gain, gate_part, weights, decay, past_k, past_v, memory):
    seqs, heads, dk, dv = memory.shape
    rows, local = tokens.shape
    width, cols = weights[0].shape
    return pl.pallas_call(
        functools.partial(project_kernel, n, m, squares_at, local * m),
        out_shape=[jax.ShapeDtypeStruct((rows, cols), jnp.bfloat16)] * 4
        + [
            jax.ShapeDtypeStruct(gate_part.shape, jnp.float32),
            jax.ShapeDtypeStruct((rows, heads * dv), jnp.float32),
            jax.ShapeDtypeStruct(memory.shape, jnp.float32),
        ],
        in_specs=[vmem] * 7
        + [pl.BlockSpec(memory_space=pltpu.SMEM), vmem, vmem]
        + [pl.BlockSpec(memory_space=pltpu.HBM)],
        out_specs=[vmem] * 6 + [pl.BlockSpec(memory_space=pltpu.HBM)],
        scratch_shapes=[
            pltpu.VMEM((n, rows, width), jnp.bfloat16),
            pltpu.VMEM((4, n, rows, cols), jnp.bfloat16),
            pltpu.VMEM((4, n // 2, rows, cols), jnp.bfloat16),
            pltpu.VMEM((4, n // 2, rows, cols), jnp.bfloat16),
            pltpu.VMEM((4, n // 2 - 1, rows, cols), jnp.bfloat16),
            pltpu.VMEM((m - 1,) + gate_part.shape, jnp.float32),
            pltpu.VMEM(memory.shape, jnp.float32),
            pltpu.VMEM(memory.shape, jnp.bfloat16),
            pltpu.SemaphoreType.DMA((n,)),
            pltpu.SemaphoreType.DMA((n,)),
            pltpu.SemaphoreType.DMA((4, n // 2)),
            pltpu.SemaphoreType.DMA((4, n // 2)),
            pltpu.SemaphoreType.DMA((4, n // 2 - 1)),
            pltpu.SemaphoreType.DMA((4, n // 2 - 1)),
            pltpu.SemaphoreType.DMA((m - 1,)),
            pltpu.SemaphoreType.DMA((m - 1,)),
            pltpu.SemaphoreType.DMA((seqs,)),
            pltpu.SemaphoreType.DMA((seqs,)),
        ],
        compiler_params=pltpu.CompilerParams(collective_id=0, has_side_effects=True),
    )(tokens, gain, gate_part, *weights, decay, past_k, past_v, memory)


def mix_kernel(n, m, gated, w, out, g_buf, p_buf, q_buf, g_send, g_recv, p_send, p_recv):
    k = lax.axis_index("kv")
    t = lax.axis_index("tp")
    r = n // m
    rows = g_buf.shape[1]
    width = w.shape[1]
    t0 = k // r
    mine = k % r
    to_self = t0 == t
    barrier = pltpu.get_barrier_semaphore()

    def source(q):
        h = q // m
        return t * r + h, q % m

    def is_self(kk, tt):
        return jnp.logical_and(kk == k, tt == t)

    each(n, lambda i: signal(barrier, lax.rem(k + i, n), t), 1)

    def greet_source(q):
        kk, tt = source(q)

        @pl.when(jnp.logical_not(is_self(kk, tt)))
        def _():
            signal(barrier, kk, tt)

    each(n, greet_source)
    pl.semaphore_wait(barrier, (n - 1) + n - to_self.astype(jnp.int32))

    half = n // 2
    z = k // 2
    x = k % 2
    beside = z * 2 + 1 - x

    def along_copy(i):
        to = lax.rem(z + i, half) * 2 + x
        return remote(gated, g_buf.at[k], g_send.at[i], g_recv.at[k], to, t)

    def across_copy(i):
        at = lax.rem(z + half - i, half) * 2 + x
        return remote(g_buf.at[at], g_buf.at[at], g_send.at[half + i], g_recv.at[at], beside, t)

    own_copy = remote(gated, g_buf.at[k], g_send.at[0], g_recv.at[k], beside, t)
    each(half, lambda i: along_copy(i).start(), 1)
    own_copy.start()
    g_buf[k] = gated[...]

    def landed(at):
        remote(gated, g_buf.at[at], g_send.at[0], g_recv.at[at], k, t).wait_recv()

    def hand_on(i):
        landed(lax.rem(z + half - i, half) * 2 + x)
        across_copy(i).start()

    each(half, hand_on, 1)
    each(half, lambda i: landed(i * 2 + 1 - x))
    part = jnp.dot(
        g_buf[...].reshape(n * rows, -1), w[...], preferred_element_type=jnp.float32
    )
    p_buf[...] = part.astype(jnp.bfloat16).reshape(n, rows, width)

    def part_copy(i):
        to = lax.rem(k + n - i, n)
        return remote(
            p_buf.at[to],
            q_buf.at[mine * m + t],
            p_send.at[i],
            p_recv.at[mine * m + t],
            to,
            t0,
        )

    each(n, lambda i: part_copy(i).start(), 1)

    @pl.when(jnp.logical_not(to_self))
    def _():
        part_copy(0).start()

    @pl.when(to_self)
    def _():
        q_buf[mine * m + t] = p_buf[k]

    def wait_part(q):
        kk, tt = source(q)

        @pl.when(jnp.logical_not(is_self(kk, tt)))
        def _():
            remote(p_buf.at[0], q_buf.at[q], p_send.at[0], p_recv.at[q], k, t).wait_recv()

    each(n, wait_part)
    for h in range(r):
        total = q_buf[h * m].astype(jnp.float32)
        for j in range(1, m):
            total = total + q_buf[h * m + j].astype(jnp.float32)
        out[:, h * width : (h + 1) * width] = total.astype(jnp.bfloat16)

    each(half, lambda i: along_copy(i).wait_send(), 1)
    own_copy.wait_send()
    each(half, lambda i: across_copy(i).wait_send(), 1)
    each(n, lambda i: part_copy(i).wait_send(), 1)

    @pl.when(jnp.logical_not(to_self))
    def _():
        part_copy(0).wait_send()


def mix(n, m, gated, weight):
    rows, depth = gated.shape
    width = weight.shape[1]
    return pl.pallas_call(
        functools.partial(mix_kernel, n, m),
        out_shape=jax.ShapeDtypeStruct((rows, width * n // m), jnp.bfloat16),
        in_specs=[vmem] * 2,
        out_specs=vmem,
        scratch_shapes=[
            pltpu.VMEM((n, rows, depth), jnp.bfloat16),
            pltpu.VMEM((n, rows, width), jnp.bfloat16),
            pltpu.VMEM((n, rows, width), jnp.bfloat16),
            pltpu.SemaphoreType.DMA((n,)),
            pltpu.SemaphoreType.DMA((n,)),
            pltpu.SemaphoreType.DMA((n,)),
            pltpu.SemaphoreType.DMA((n,)),
        ],
        compiler_params=pltpu.CompilerParams(collective_id=1, has_side_effects=True),
    )(gated, weight)


def body(
    n,
    m,
    tokens,
    norm_gain,
    query_weight,
    key_weight,
    value_weight,
    outgate_weight,
    ingate_weight,
    forget_weight,
    forget_bias,
    output_weight,
    state_memory,
    state_normaliser,
    state_stabiliser,
    past_keys,
    past_values,
    past_ingate,
    past_forget,
    accepted,
):
    seq_count, head_count = state_stabiliser.shape
    tok_rows, local = tokens.shape
    chain_len = past_keys.shape[1]
    all_heads = ingate_weight.shape[1]
    tp_at = lax.axis_index("tp")
    own_part = tokens.astype(jnp.float32)
    squares = jnp.sum(own_part * own_part, axis=1, keepdims=True)
    own_gain = lax.dynamic_slice_in_dim(norm_gain, tp_at * local, local, 0)
    gate_weight = jnp.concatenate(
        [
            lax.dynamic_slice_in_dim(w, tp_at * local, local, 0)
            for w in (ingate_weight, forget_weight)
        ],
        axis=1,
    ).astype(jnp.float32)
    raw = jnp.dot(
        own_part * own_gain,
        gate_weight,
        precision=lax.Precision.HIGHEST,
        preferred_element_type=jnp.float32,
    )
    lanes = -(-(2 * all_heads + 1) // 128) * 128
    gate_part = jnp.concatenate(
        [raw, squares, jnp.zeros((tok_rows, lanes - 2 * all_heads - 1), jnp.float32)], axis=1
    )
    key_scale = (past_keys.shape[2] // head_count) ** (-0.5)
    taken_mask = jnp.arange(chain_len)[None, None, :] < accepted[:, None, None]
    decay, weighted, normaliser, stabiliser = catch_up(
        state_normaliser,
        state_stabiliser,
        heads_view(past_keys, seq_count, head_count) * key_scale,
        past_ingate.transpose(0, 2, 1),
        past_forget.transpose(0, 2, 1),
        taken_mask,
    )
    past_k = weighted.transpose(0, 2, 1, 3).reshape(past_keys.shape).astype(jnp.bfloat16)
    query_b, key_b, value_b, outgate_b, gates, from_memory, memory = project(
        n,
        m,
        2 * all_heads,
        tokens,
        norm_gain[None, :],
        gate_part,
        (query_weight, key_weight, value_weight, outgate_weight),
        decay.reshape(-1),
        past_k,
        past_values,
        state_memory,
    )
    first_head = tp_at * head_count
    in_gate = lax.dynamic_slice_in_dim(gates, first_head, head_count, 1)
    bias_own = lax.dynamic_slice_in_dim(forget_bias, first_head, head_count, 0)
    forget_pre = lax.dynamic_slice_in_dim(gates, all_heads + first_head, head_count, 1) + bias_own
    hidden = advance(
        heads_view(from_memory, seq_count, head_count),
        normaliser,
        stabiliser,
        heads_view(query_b, seq_count, head_count),
        heads_view(key_b, seq_count, head_count) * key_scale,
        heads_view(value_b, seq_count, head_count),
        in_gate.reshape(seq_count, chain_len, head_count).transpose(0, 2, 1),
        forget_pre.reshape(seq_count, chain_len, head_count).transpose(0, 2, 1),
    )
    gated_heads = jax.nn.sigmoid(heads_view(outgate_b, seq_count, head_count)) * hidden
    gated_rows = gated_heads.transpose(0, 2, 1, 3).reshape(tok_rows, -1).astype(jnp.bfloat16)
    result = mix(n, m, gated_rows, output_weight)
    return (result, memory, normaliser, stabiliser, key_b, value_b)


def solution(mesh):
    placed = (
        P("kv", "tp"),
        P(),
        P("kv", "tp"),
        P("kv", "tp"),
        P("kv", "tp"),
        P("kv", "tp"),
        P(),
        P(),
        P(),
        P("tp", "kv"),
        P("kv", "tp", None, None),
        P("kv", "tp", None),
        P("kv", "tp"),
        P("kv", None, "tp"),
        P("kv", None, "tp"),
        P("kv", None, "tp"),
        P("kv", None, "tp"),
        P("kv"),
    )
    return jax.shard_map(
        functools.partial(body, mesh.shape["kv"], mesh.shape["tp"]),
        mesh=mesh,
        in_specs=placed,
        out_specs=(
            P("kv", "tp"),
            P("kv", "tp", None, None),
            P("kv", "tp", None),
            P("kv", "tp"),
            P("kv", "tp"),
            P("kv", "tp"),
        ),
        check_vma=False,
    )
```

profile of v0, /device:TPU:5, one launch (start us, length us, event | category | flops | bytes accessed | tf_op | source)
XLA Modules:
  0.0 109.9 jit_solution(1956220323029509835)
XLA Ops:
  0.6 0.7 dynamic_slice.22
  1.4 0.7 iota_compare_fusion.1
  2.0 1.0 fusion.1
  3.1 0.8 copy.130
  3.8 0.7 dynamic_slice.18
  4.5 0.7 negate_bitcast_fusion
  5.3 0.7 fusion.20
  6.0 0.7 fusion.39
  6.7 0.1 copy.165
  7.0 0.6 reshape.103.decay
  7.6 0.8 exponential_multiply_fusion
  8.4 0.1 copy.154
  8.5 0.1 copy.123
  8.6 0.1 copy.135
  8.7 0.8 constant_dynamic-slice_fusion.1
  9.4 1.0 fusion
  10.5 0.7 maximum_maximum_fusion.gate_part
  11.2 0.1 mul.98
  11.3 0.1 mul.99
  11.4 1.5 %multiply_convert_fusion.past_k = bf16[8,4,1024]{2,1,0:T(4,128)(2,1)} fusion(f32[8,4,1024]{2,1,0:T(4,128)S(1)} %mul.99, bf16[8,4,1024]{2,1,0:T(4,128)(2,1)} %param.31), kind=kLoop, calls=%fused_computation.17 | loop fusion | flops 98304 | bytes 262144 | tf_op jit(solution)/shard_map/convert_element_type | solution.py:473
  12.9 0.9 reshape.109
  13.8 0.1 fusion.2
  13.9 0.8 multiply_add_fusion
  14.7 51.2 %shard_map.217 = (bf16[32,1024]{1,0:T(8,128)(2,1)}, bf16[32,1024]{1,0:T(8,128)(2,1)}, bf16[32,1024]{1,0:T(8,128)(2,1)}, bf16[32,1024]{1,0:T(8,128)(2,1)}, f32[32...) custom-call(bf16[32,1024]{1,0:T(8,128)(2,1)} %tok.1, f32[1,4096]{1,0:T(1,128)} %bitcast.95, ...), custom_call_target="tpu_custom_call" | custom-call | tf_op jit(solution)/shard_map/pallas_call | solution.py:252
  65.9 0.9 add_negate_fusion
  66.8 0.1 copy.138
  67.0 0.1 copy.164
  67.1 0.1 copy.140
  67.2 0.2 fusion.15
  67.4 0.1 copy.144
  67.5 0.1 copy.150
  67.6 0.9 reshape.106
  68.5 0.1 multiply_reduce_fusion
  68.6 0.1 copy.155
  68.7 0.9 add_divide_fusion
  69.7 0.9 convert_multiply_fusion.3
  70.6 0.2 fusion.41
  70.8 0.1 copy.156
  71.0 0.9 reshape.107
  71.8 0.2 fusion.11
  72.1 1.0 reshape.105
  73.0 0.2 fusion.5
  73.3 0.6 copy.173
  73.9 25.5 %shard_map.218 = bf16[32,1024]{1,0:T(8,128)(2,1)} custom-call(bf16[32,1024]{1,0:T(8,128)(2,1)} %bitcast.86, bf16[1024,512]{1,0:T(8,128)(2,1)} %w.1), custom_call_target="tpu_custom_call" | custom-call | tf_op jit(solution)/shard_map/pallas_call | solution.py:398
  99.5 1.5 %copy.212 = bf16[32,1024]{1,0:T(8,128)(2,1)} copy(bf16[32,1024]{1,0:T(8,128)(2,1)} %shard_map.218) | data formatting | bytes 131072
  101.0 7.7 %copy.213 = f32[8,4,256,256]{3,2,1,0:T(8,128)} copy(f32[8,4,256,256]{3,2,1,0:T(8,128)} %get-tuple-element.53) | data formatting | bytes 16777216
  108.7 0.6 copy.214
  109.3 0.6 copy.215
  (28 shorter events, 0.5 us)
Async XLA Ops:
  7.0 63.9 %copy-start.3 = (f32[8,4]{0,1:T(4,128)}, f32[8,4]{0,1:T(4,128)S(1)}, u32[]{:S(2)}) copy-start(f32[8,4]{0,1:T(4,128)S(1)} %copy.134) | copy-start | bytes 388
  14.7 84.8 %copy-start.2 = (f32[8,4,256]{2,1,0:T(4,128)}, f32[8,4,256]{2,1,0:T(4,128)S(1)}, u32[]{:S(2)}) copy-start(f32[8,4,256]{2,1,0:T(4,128)S(1)} %multiply_add_fusion) | copy-start | bytes 98308
  101.0 7.7 %copy-start.1 = (bf16[32,1024]{1,0:T(8,128)(2,1)S(1)}, bf16[32,1024]{1,0:T(8,128)(2,1)}, u32[]{:S(2)}) copy-start(bf16[32,1024]{1,0:T(8,128)(2,1)} %get-tuple-element.56) | copy-start | bytes 196612
  101.0 8.3 %copy-start = (bf16[32,1024]{1,0:T(8,128)(2,1)S(1)}, bf16[32,1024]{1,0:T(8,128)(2,1)}, u32[]{:S(2)}) copy-start(bf16[32,1024]{1,0:T(8,128)(2,1)} %get-tuple-element.57) | copy-start | bytes 196612
where the time goes:
time: 111 us; the launch traced here: 110 us
  Pallas kernels  76.7 us (69%)
  local copies, waits for them, and re-layouts  20 us (18%)
  other arithmetic  11 us (10%)
  matrix products  1.48 us (1%)
    pallas_call x1, Pallas kernels, project(): pl.pallas_call(functools.partial(project_kernel, n, m, squares_at, local...  51.2 us
    pallas_call x1, Pallas kernels, mix(): pl.pallas_call(functools.partial(mix_kernel, n, m), out_shape=jax.ShapeDt...  25.5 us
    unnamed x16, local copies, waits for them, and re-layouts  11.9 us
    reshape x4, local copies, waits for them, and re-layouts, heads_view(): rows.astype(jnp.float32)  3.61 us

commit v1 on v0

v1 whole, which is shorter than its diff:
```python
import functools

import jax
import jax.numpy as jnp
from jax import lax
from jax.experimental import pallas as pl
from jax.experimental.pallas import tpu as pltpu
from jax.sharding import PartitionSpec as P

epsilon = 1e-06
MESH = pl.DeviceIdType.MESH
vmem = pl.BlockSpec(memory_space=pltpu.VMEM)
hbm = pl.BlockSpec(memory_space=pltpu.HBM)
f32 = jnp.float32
bf16 = jnp.bfloat16
DMA = pltpu.SemaphoreType.DMA


def signal(sem, kv, tp):
    pl.semaphore_signal(sem, inc=1, device_id={"kv": kv, "tp": tp}, device_id_type=MESH)


def remote(src, dst, send_sem, recv_sem, kv, tp):
    return pltpu.make_async_remote_copy(
        src_ref=src,
        dst_ref=dst,
        send_sem=send_sem,
        recv_sem=recv_sem,
        device_id={"kv": kv, "tp": tp},
        device_id_type=MESH,
    )


def each(count, step, start=0):
    def run(index, carry):
        step(index)
        return carry

    lax.fori_loop(start, count, run, 0)


def log_sigmoid(v):
    return jnp.minimum(v, 0.0) - jnp.log1p(jnp.exp(-jnp.abs(v)))


def iota(shape, axis):
    return lax.broadcasted_iota(jnp.int32, shape, axis)


def cell_kernel(
    n, m, all_heads, features, chain,
    tok_h, gain_h, wi_h, wf_h, bias_h, w0_h, w1_h, w2_h, w3_h, wo_h,
    memory_h, norm_h, stab_h, past_k_h, past_v_h, past_i_h, past_f_h, taken_h,
    mixed, key_b, value_b, memory, norm_new, stab_new,
    tok, gain, wg, bias, w_in, w_out, norm, stab, past_k, past_v, past_i, past_f, taken,
    x_buf, xs, keep, give, near, pair, far, g_own, g_buf,
    m_low, weights, decay, query_b, outgate_b, from_memory, gated,
    a_buf, p_buf, q_buf, o_send, o_buf,
    in_sem, w_sem, m_sem, t_send, f_send, x_recv, g_send, g_recv,
    n_send, n_recv, z_send, z_recv, a_send, a_recv, p_send, p_recv, o_ssem, o_rsem,
):
    k = lax.axis_index("kv")
    t = lax.axis_index("tp")
    r = n // m
    half = n // 2
    pairs = m // 2
    rows, local = tok.shape
    width = xs.shape[2]
    cols = w_in.shape[2]
    out_cols = w_out.shape[1]
    seqs, heads, dk, dv = memory.shape
    z = k // 2
    x = k % 2
    core = t % 2
    partner = t + 1 - 2 * core
    beside = z * 2 + 1 - x
    t0 = k // r
    mine = k % r
    root = t0 == t
    root_core = t0 % 2 == core
    turn = 1 - 2 * (z // max(half // 2, 1))

    def plane(i):
        return lax.rem(z + i * turn + half, half)

    small = [
        pltpu.make_async_copy(tok_h, tok, in_sem.at[0]),
        pltpu.make_async_copy(gain_h, gain, in_sem.at[1]),
        pltpu.make_async_copy(
            wi_h.at[:, pl.ds(pl.multiple_of(t * local, local), local)],
            wg.at[pl.ds(0, all_heads)], in_sem.at[2],
        ),
        pltpu.make_async_copy(
            wf_h.at[:, pl.ds(pl.multiple_of(t * local, local), local)],
            wg.at[pl.ds(all_heads, all_heads)], in_sem.at[3],
        ),
    ]
    late = [
        pltpu.make_async_copy(src, dst, in_sem.at[4 + i])
        for i, (src, dst) in enumerate((
            (bias_h, bias), (norm_h, norm), (stab_h, stab), (past_k_h, past_k),
            (past_v_h, past_v), (past_i_h, past_i), (past_f_h, past_f), (taken_h, taken),
        ))
    ]
    big = [
        pltpu.make_async_copy(src, w_in.at[i], w_sem.at[i])
        for i, src in enumerate((w0_h, w1_h, w2_h, w3_h))
    ]
    load_out = pltpu.make_async_copy(wo_h, w_out, w_sem.at[4])

    def load(q):
        return pltpu.make_async_copy(memory_h.at[q], memory.at[q], m_sem.at[q])

    for copy in small + big + late:
        copy.start()
    load_out.start()
    each(seqs, lambda q: load(q).start())

    barrier = pltpu.get_barrier_semaphore()
    each(n, lambda i: signal(barrier, lax.rem(k + i, n), t), 1)
    each(m, lambda j: signal(barrier, k, lax.rem(t + j, m)), 1)
    last_at = k % m

    def greet_last(h):
        kk = t * r + h

        @pl.when(jnp.logical_not(jnp.logical_and(kk == k, last_at == t)))
        def _():
            signal(barrier, kk, last_at)

    each(r, greet_last)
    both = jnp.logical_and(root, last_at == t).astype(jnp.int32)
    pl.semaphore_wait(barrier, (n - 1) + (m - 1) + r - both)

    small[0].wait()

    def token_copy(h):
        cut = pl.ds(pl.multiple_of(h * width, width), width)
        return remote(tok.at[:, cut], x_buf.at[k], t_send.at[h], x_recv.at[k], t * r + h, t)

    def own_token(h):
        return jnp.logical_and(root, h == mine)

    def start_token(h):
        @pl.when(jnp.logical_not(own_token(h)))
        def _():
            token_copy(h).start()

    each(r, start_token)

    @pl.when(root)
    def _():
        x_buf[k] = tok[:, pl.ds(pl.multiple_of(mine * width, width), width)]

    def forward(j, i, to):
        return remote(x_buf.at[j], x_buf.at[j], f_send.at[i, j], x_recv.at[j], k, to)

    def cousin(i):
        return lax.rem(t + 2 * i, m)

    def pass_token(j):
        @pl.when(jnp.logical_not(jnp.logical_and(root, j == k)))
        def _():
            remote(
                tok.at[:, pl.ds(0, width)], x_buf.at[j], t_send.at[0], x_recv.at[j], k, t
            ).wait_recv()

        @pl.when(root)
        def _():
            for i in range(1, pairs):
                forward(j, i, cousin(i)).start()

        @pl.when(root_core)
        def _():
            forward(j, 0, partner).start()

    wg[pl.ds(2 * all_heads, wg.shape[0] - 2 * all_heads), :] = jnp.zeros(
        (wg.shape[0] - 2 * all_heads, local), bf16
    )
    for copy in small[1:]:
        copy.wait()
    floats = tok[...].astype(f32)
    squares = jnp.sum(floats * floats, axis=1, keepdims=True)
    lifted = floats * gain[:, pl.ds(pl.multiple_of(t * local, local), local)]
    raw = lax.dot_general(
        lifted.astype(bf16), wg[...], (((1,), (1,)), ((), ())), preferred_element_type=f32
    )
    lane = iota(raw.shape, 1)
    g_own[...] = jnp.where(lane < 2 * all_heads, raw, squares)

    def gate_copy(j):
        return remote(
            g_own, g_buf.at[j - 1], g_send.at[j - 1], g_recv.at[j - 1], k, lax.rem(t + j, m)
        )

    each(m, lambda j: gate_copy(j).start(), 1)
    own_gain = gain[:, pl.ds(pl.multiple_of(k * width, width), width)]

    def scale_plane(p):
        for side, j in enumerate((p * 2 + x, p * 2 + 1 - x)):
            xs[p, side * rows : (side + 1) * rows, :] = (
                x_buf[j].astype(f32) * own_gain
            ).astype(bf16)

    def near_copy(c, p):
        return remote(
            give.at[c, p], near.at[c, p], n_send.at[c, p], n_recv.at[c, p], beside, t
        )

    def project(c, p):
        part = jnp.dot(xs[p], w_in[c], preferred_element_type=f32)
        give[c, p] = part[rows:].astype(bf16)
        near_copy(c, p).start()
        keep[c, p] = part[:rows].astype(bf16)

    def take_plane(p):
        pass_token(p * 2 + x)
        pass_token(p * 2 + 1 - x)
        scale_plane(p)

    take_plane(z)
    for c in range(2):
        big[c].wait()
        project(c, z)
    for c in range(2, 4):
        big[c].wait()

    def far_plane(i):
        p = plane(i)
        take_plane(p)
        for c in range(4):
            project(c, p)

    each(half, far_plane, 1)
    for c in range(2, 4):
        project(c, z)

    for copy in late:
        copy.wait()
    key_scale = dk ** (-0.5)
    reach = taken[...]
    chain_sum = jnp.zeros((heads, seqs), f32)
    running = []
    for j in range(chain):
        chain_sum = chain_sum + jnp.where(j < reach, log_sigmoid(past_f[j]), 0.0)
        running.append(chain_sum)
    carried_log = chain_sum + stab[...]
    new_stab = carried_log
    ends = []
    for j in range(chain):
        ends.append(jnp.where(j < reach, chain_sum - running[j] + past_i[j], -jnp.inf))
        new_stab = jnp.maximum(new_stab, ends[j])
    stab_new[...] = new_stab
    decay[...] = jnp.exp(carried_log - new_stab)
    for j in range(chain):
        weight_j = jnp.exp(ends[j] - new_stab)
        for h in range(heads):
            weights[h, j : j + 1, :] = weight_j[h : h + 1, :]

    def take(q):
        load(q).wait()
        for h in range(heads):
            at = slice(h * dk, (h + 1) * dk)
            w_col = jnp.sum(
                jnp.where(iota((chain, seqs), 1) == q, weights[h], 0.0), axis=1, keepdims=True
            )
            fade = jnp.sum(
                jnp.where(iota((1, seqs), 1) == q, decay[h : h + 1, :], 0.0),
                axis=1, keepdims=True,
            )
            lifted_k = past_k[q, :, at].astype(f32) * key_scale * w_col
            norm_new[q, h : h + 1, :] = fade * norm[q, h : h + 1, :] + jnp.sum(
                lifted_k, axis=0, keepdims=True
            )
            added = lax.dot_general(
                lifted_k.astype(bf16),
                past_v[q, :, h * dv : (h + 1) * dv],
                (((0,), (0,)), ((), ())),
                preferred_element_type=f32,
            )
            new = fade * memory[q, h] + added
            memory[q, h] = new
            m_low[q, h] = new.astype(bf16)

    def fold(c, p):
        near_copy(c, p).wait_recv()
        pair[c, p] = (keep[c, p].astype(f32) + near[c, p].astype(f32)).astype(bf16)

    def far_copy(c, p):
        slot = lax.rem(z - p + half, half) - 1
        return remote(
            pair.at[c, p], far.at[c, slot], z_send.at[c, p], z_recv.at[c, slot], p * 2 + x, t
        )

    def fold_plane(i):
        p = plane(i)
        each(seqs * i // (half - 1), take, seqs * (i - 1) // (half - 1))
        for c in range(4):
            fold(c, p)
            far_copy(c, p).start()

    for c in range(2):
        fold(c, z)
    each(half, fold_plane, 1)

    def landed_far(c, i):
        remote(
            pair.at[c, 0], far.at[c, i], z_send.at[c, 0], z_recv.at[c, i], k, t
        ).wait_recv()

    each(m, lambda j: gate_copy(j).wait_recv(), 1)
    total = g_own[...]
    for j in range(m - 1):
        total = total + g_buf[j]
    scale = lax.rsqrt(total[:, 2 * all_heads : 2 * all_heads + 1] / features + epsilon)
    gates = total * scale

    def settle(c, out):
        each(half - 1, lambda i: landed_far(c, i))
        summed = pair[c, z].astype(f32)
        for i in range(half - 1):
            summed = summed + far[c, i].astype(f32)
        out[...] = (summed * scale).astype(bf16)

    settle(0, query_b)
    row_seq = iota((rows, dv), 0) // chain
    from_memory[...] = jnp.zeros(from_memory.shape, f32)

    def recall(q):
        for h in range(heads):
            at = slice(h * dv, (h + 1) * dv)
            got = jnp.dot(
                query_b[:, h * dk : (h + 1) * dk], m_low[q, h], preferred_element_type=f32
            )
            from_memory[:, at] = jnp.where(row_seq == q, got, from_memory[:, at])

    each(seqs, recall)
    settle(1, key_b)

    token_row = iota((rows, rows), 0)
    token_col = iota((rows, rows), 1)
    same_seq = token_row // chain == token_col // chain
    causal = jnp.logical_and(same_seq, token_col <= token_row)
    diagonal = token_row == token_col
    own_seq = iota((rows, seqs), 0) // chain == iota((rows, seqs), 1)
    first = t * heads

    def to_row(col):
        return jnp.sum(jnp.where(diagonal, col, 0.0), axis=0, keepdims=True)

    def pick(array, at):
        return jnp.sum(
            jnp.where(iota(array.shape, 1) == at, array, 0.0), axis=1, keepdims=True
        )

    scores, carries, dens = [], [], []
    for h in range(heads):
        at = slice(h * dk, (h + 1) * dk)
        in_col = pick(gates, first + h)
        forget = pick(gates, all_heads + first + h) + pick(bias[...], first + h)
        b_col = jnp.sum(
            jnp.where(causal, to_row(log_sigmoid(forget)), 0.0), axis=1, keepdims=True
        )
        within = jnp.where(causal, b_col + to_row(in_col - b_col), -jnp.inf)
        stab_col = jnp.sum(
            jnp.where(own_seq, stab_new[h : h + 1, :], 0.0), axis=1, keepdims=True
        )
        carried = b_col + stab_col
        stable = jnp.maximum(carried, jnp.max(within, axis=1, keepdims=True))
        carry = jnp.exp(carried - stable)
        match = lax.dot_general(
            query_b[:, at], key_b[:, at], (((1,), (1,)), ((), ())), preferred_element_type=f32
        )
        score = match * key_scale * jnp.exp(within - stable)
        across_n = lax.dot_general(
            query_b[:, at].astype(f32), norm_new[:, h, :], (((1,), (1,)), ((), ())),
            precision=lax.Precision.HIGHEST, preferred_element_type=f32,
        )
        q_n = jnp.sum(jnp.where(own_seq, across_n, 0.0), axis=1, keepdims=True)
        den = carry * q_n + jnp.sum(score, axis=1, keepdims=True)
        scores.append(score.astype(bf16))
        carries.append(carry)
        dens.append(1.0 / jnp.maximum(jnp.abs(den), 1.0))

    for c in range(2, 4):
        fold(c, z)
    settle(2, value_b)
    for h in range(heads):
        at = slice(h * dv, (h + 1) * dv)
        fresh = jnp.dot(scores[h], value_b[:, at], preferred_element_type=f32)
        from_memory[:, at] = (carries[h] * from_memory[:, at] + fresh) * dens[h]
    settle(3, outgate_b)
    gated[...] = (jax.nn.sigmoid(outgate_b[...].astype(f32)) * from_memory[...]).astype(bf16)

    def along_copy(i):
        return remote(gated, a_buf.at[k], a_send.at[i], a_recv.at[k], plane(i) * 2 + x, t)

    def across_copy(i):
        at = plane(i) * 2 + x
        return remote(
            a_buf.at[at], a_buf.at[at], a_send.at[half + i], a_recv.at[at], beside, t
        )

    own_copy = remote(gated, a_buf.at[k], a_send.at[0], a_recv.at[k], beside, t)
    each(half, lambda i: along_copy(i).start(), 1)
    own_copy.start()
    a_buf[k] = gated[...]
    load_out.wait()

    def landed(at):
        remote(gated, a_buf.at[at], a_send.at[0], a_recv.at[at], k, t).wait_recv()

    def part_copy(kb):
        j = kb // m
        return remote(p_buf.at[kb], q_buf.at[j, t], p_send.at[kb], p_recv.at[j, t], k, kb % m)

    def away(kb):
        return kb % m != t

    def mix_plane(p):
        landed(p * 2 + 1 - x)
        both_rows = a_buf[pl.ds(p * 2, 2)].reshape(2 * rows, cols)
        part = jnp.dot(both_rows, w_out[...], preferred_element_type=f32).astype(bf16)
        for side in range(2):
            kb = p * 2 + side
            p_buf[kb] = part[side * rows : (side + 1) * rows]

            @pl.when(away(kb))
            def _():
                part_copy(kb).start()

    def step_plane(i):
        landed(plane(i) * 2 + x)
        across_copy(i).start()
        mix_plane(plane(i - 1))

    each(half, step_plane, 1)
    mix_plane(plane(half - 1))

    def final_copy(j):
        return remote(o_send.at[j], o_buf.at[mine], o_ssem.at[j], o_rsem.at[mine], j * m + t, t0)

    def stays(j):
        return jnp.logical_and(root, j * m + t == k)

    for j in range(r):
        def landed_part(tt, j=j):
            @pl.when(tt != t)
            def _():
                remote(
                    p_buf.at[0], q_buf.at[j, tt], p_send.at[0], p_recv.at[j, tt], k, t
                ).wait_recv()

        each(m, landed_part)
        q_buf[j, t] = p_buf[j * m + t]
        summed = q_buf[j, 0].astype(f32)
        for tt in range(1, m):
            summed = summed + q_buf[j, tt].astype(f32)
        o_send[j] = summed.astype(bf16)

        @pl.when(jnp.logical_not(stays(j)))
        def _(j=j):
            final_copy(j).start()

        @pl.when(stays(j))
        def _(j=j):
            o_buf[mine] = o_send[j]

    for h in range(r):
        @pl.when(jnp.logical_not(jnp.logical_and(t * r + h == k, last_at == t)))
        def _(h=h):
            remote(
                o_send.at[0], o_buf.at[h], o_ssem.at[0], o_rsem.at[h], k, t
            ).wait_recv()

        mixed[:, h * out_cols : (h + 1) * out_cols] = o_buf[h]

    def drain_token(h):
        @pl.when(jnp.logical_not(own_token(h)))
        def _():
            token_copy(h).wait_send()

    each(r, drain_token)

    def drain_forward(j):
        @pl.when(root)
        def _():
            for i in range(1, pairs):
                forward(j, i, cousin(i)).wait_send()

        @pl.when(root_core)
        def _():
            forward(j, 0, partner).wait_send()

    each(n, drain_forward)
    each(m, lambda j: gate_copy(j).wait_send(), 1)
    for c in range(4):
        each(half, lambda p, c=c: near_copy(c, p).wait_send())
        each(half, lambda i, c=c: far_copy(c, plane(i)).wait_send(), 1)
    each(half, lambda i: along_copy(i).wait_send(), 1)
    own_copy.wait_send()
    each(half, lambda i: across_copy(i).wait_send(), 1)

    def drain_part(kb):
        @pl.when(away(kb))
        def _():
            part_copy(kb).wait_send()

    each(n, drain_part)
    for j in range(r):
        @pl.when(jnp.logical_not(stays(j)))
        def _(j=j):
            final_copy(j).wait_send()


def cell(n, m, tokens, gain, wi, wf, bias, weights, w_out, memory, norm, stab, past_k, past_v,
         past_i, past_f, taken):
    seqs, heads, dk, dv = memory.shape
    rows, local = tokens.shape
    width, cols = weights[0].shape
    all_heads = wi.shape[0]
    chain = past_k.shape[1]
    depth, out_cols = w_out.shape
    half, r = n // 2, n // m
    lanes = -(-(2 * all_heads + 1) // 128) * 128
    row_block = jax.ShapeDtypeStruct((rows, cols), bf16)
    V = pltpu.VMEM
    outs = [
        V((rows, local), bf16), V((rows, cols), bf16), V((rows, cols), bf16),
        V(memory.shape, f32), V(norm.shape, f32), V(stab.shape, f32),
    ]
    return pl.pallas_call(
        functools.partial(cell_kernel, n, m, all_heads, local * m, chain),
        out_shape=outs,
        in_specs=[hbm] * 18,
        out_specs=[vmem] * 6,
        scratch_shapes=[
            V((rows, local), bf16), V(gain.shape, f32), V((lanes, local), bf16),
            V(bias.shape, f32), V((4, width, cols), bf16), V(w_out.shape, bf16),
            V(norm.shape, f32), V(stab.shape, f32), V(past_k.shape, bf16),
            V(past_v.shape, bf16), V(past_i.shape, f32), V(past_f.shape, f32),
            V(taken.shape, jnp.int32),
            V((n, rows, width), bf16), V((half, 2 * rows, width), bf16),
            V((4, half, rows, cols), bf16), V((4, half, rows, cols), bf16),
            V((4, half, rows, cols), bf16), V((4, half, rows, cols), bf16),
            V((4, half - 1, rows, cols), bf16),
            V((rows, lanes), f32), V((m - 1, rows, lanes), f32),
            V(memory.shape, bf16), V((heads, chain, seqs), f32), V(stab.shape, f32),
            V((rows, cols), bf16), V((rows, cols), bf16), V((rows, cols), f32),
            V((rows, cols), bf16),
            V((n, rows, cols), bf16), V((n, rows, out_cols), bf16),
            V((r, m, rows, out_cols), bf16), V((r, rows, out_cols), bf16),
            V((r, rows, out_cols), bf16),
            DMA((12,)), DMA((5,)), DMA((seqs,)), DMA((r,)), DMA((m // 2, n)), DMA((n,)),
            DMA((m - 1,)), DMA((m - 1,)),
            DMA((4, half)), DMA((4, half)), DMA((4, half)), DMA((4, half - 1)),
            DMA((n,)), DMA((n,)), DMA((n,)), DMA((r, m)), DMA((r,)), DMA((r,)),
        ],
        compiler_params=pltpu.CompilerParams(
            collective_id=0, has_side_effects=True, vmem_limit_bytes=40 * 1024 * 1024
        ),
    )(*(pltpu.with_memory_space_constraint(a, pltpu.HBM) for a in (
        tokens, gain, wi, wf, bias, *weights, w_out, memory, norm, stab, past_k, past_v,
        past_i, past_f, taken,
    )))


def put_kernel(count, pieces, *refs):
    sems = refs[-1]
    copies = []
    at = 0
    for src, dst, cut in zip(refs[:count], refs[count : 2 * count], pieces):
        for piece in range(cut):
            a, b = (src.at[piece], dst.at[piece]) if cut > 1 else (src, dst)
            copies.append(pltpu.make_async_copy(a, b, sems.at[at]))
            at += 1
    for copy in copies:
        copy.start()
    for copy in copies:
        copy.wait()


def put(arrays, pieces):
    return pl.pallas_call(
        functools.partial(put_kernel, len(arrays), pieces),
        out_shape=[jax.ShapeDtypeStruct(a.shape, a.dtype) for a in arrays],
        in_specs=[vmem] * len(arrays),
        out_specs=[hbm] * len(arrays),
        scratch_shapes=[DMA((sum(pieces),))],
        compiler_params=pltpu.CompilerParams(vmem_limit_bytes=16 * 1024 * 1024),
    )(*arrays)


def body(
    n, m, tokens, norm_gain, query_weight, key_weight, value_weight, outgate_weight,
    ingate_weight, forget_weight, forget_bias, output_weight, state_memory, state_normaliser,
    state_stabiliser, past_keys, past_values, past_ingate, past_forget, accepted,
):
    outs = cell(
        n, m, tokens, norm_gain[None, :], ingate_weight.T, forget_weight.T,
        forget_bias[None, :], (query_weight, key_weight, value_weight, outgate_weight),
        output_weight, state_memory, state_normaliser, state_stabiliser.T, past_keys,
        past_values, past_ingate.transpose(1, 2, 0), past_forget.transpose(1, 2, 0),
        accepted[None, :],
    )
    mixed, keys, values, memory, normaliser, stabiliser = put(
        outs, (1, 1, 1, state_memory.shape[0], 1, 1)
    )
    return (mixed, memory, normaliser, stabiliser.T, keys, values)


def solution(mesh):
    rows = P("kv", "tp")
    chained = P("kv", None, "tp")
    return jax.shard_map(
        functools.partial(body, mesh.shape["kv"], mesh.shape["tp"]),
        mesh=mesh,
        in_specs=(
            rows, P(), rows, rows, rows, rows, P(), P(), P(), P("tp", "kv"),
            P("kv", "tp", None, None), P("kv", "tp", None), rows,
            chained, chained, chained, chained, P("kv"),
        ),
        out_specs=(
            rows, P("kv", "tp", None, None), P("kv", "tp", None), rows, rows, rows,
        ),
        check_vma=False,
    )
```

time: 111 us -> 68.3 us (0.62)
  local copies, waits for them, and re-layouts: 20 us -> 0 us
  other arithmetic: 11 us -> 0 us
  Pallas kernels: 76.7 us -> 66.6 us
  matrix products: 1.48 us -> 0 us
    unnamed x16 -> x0, local copies, waits for them, and re-layouts: 11.9 us -> none
    pallas_call x2, Pallas kernels: 76.7 us -> 66.6 us  [the longest x1 63.1 us: cell(): pl.pallas_call(functools.partial(cell_kernel, n, m, all_heads, local * m,...]
    reshape x6 -> x0, local copies, waits for them, and re-layouts: 4.34 us -> none  [the longest x4 3.61 us: heads_view(): rows.astype(jnp.float32)]
    dynamic_slice x3 -> x0, local copies, waits for them, and re-layouts: 2.2 us -> none  [the longest x1 0.78 us: body(): lax.dynamic_slice_in_dim(w, tp_at * local, local, 0)]
    convert_element_type x2 -> x0, other arithmetic: 1.74 us -> none  [the longest x1 1.51 us: body(): weighted.transpose(0, 2, 1, 3).reshape(past_keys.shape).astype(jnp.bfloat16)]
    mul x2 -> x0, other arithmetic: 1.64 us -> none  [the longest x1 0.85 us: body(): heads_view(key_b, seq_count, head_count) * key_scale]
    neg x3 -> x0, other arithmetic: 1.6 us -> none  [the longest x2 0.9 us: advance(): running = jnp.cumsum(jax.nn.log_sigmoid(forget_pre), axis=-1)]
    dot_general x3 -> x0, matrix products: 1.48 us -> none  [the longest x1 1.03 us: body(): jnp.dot(own_part * own_gain, gate_weight, precision=lax.Precision.HIGHEST...]
where the time goes in v1:
time: 68.3 us; the launch traced here: 67.3 us
  Pallas kernels  66.6 us (98%)
    pallas_call x1, Pallas kernels, cell(): pl.pallas_call(functools.partial(cell_kernel, n, m, all_heads, local * m,...  63.1 us
    pallas_call x1, Pallas kernels, put(): pl.pallas_call(functools.partial(put_kernel, len(arrays), pieces), out_sh...  3.48 us

profile of v1, /device:TPU:5, one launch (start us, length us, event | category | flops | bytes accessed | tf_op | source)
XLA Modules:
  0.0 67.3 jit_solution(2171450704513438267)
XLA Ops:
  0.6 63.1 %shard_map.217 = (bf16[32,1024]{1,0:T(8,128)(2,1)S(1)}, bf16[32,1024]{1,0:T(8,128)(2,1)S(1)}, bf16[32,1024]{1,0:T(8,128)(2,1)S(1)}, f32[8,4,256,256]{3,2,1,0:T(8...) custom-call(bf16[32,1024]{1,0:T(8,128)(2,1)} %tok_h.1, f32[1,4096]{1,0:T(1,128)} %bitcast.11, ...), custom_call_target="tpu_custom_call" | custom-call | tf_op jit(solution)/shard_map/pallas_call | solution.py:532
  63.8 3.5 %shard_map.218 = (bf16[32,1024]{1,0:T(8,128)(2,1)}, bf16[32,1024]{1,0:T(8,128)(2,1)}, bf16[32,1024]{1,0:T(8,128)(2,1)}, f32[8,4,256,256]{3,2,1,0:T(8,128)}, f32[8,4,256]{2,1,0:T(4,128)}, /*index=5*/f32[4,8]{1,0:T(4,128)}) custom-call(bf16[32,1024]{1,0:T(8,128)(2,1)S(1)} %get-tuple-element.18.refs_0_, bf16[32,1024]{1,0:T(8,128)(2,1)S(1)} %get-tuple-element.19.refs_1_, ...), custom_call_target="tpu_custom_call" | custom-call | tf_op jit(solution)/shard_map/pallas_call | solution.py:584

commit v2 on v1

--- a/solution.py
+++ b/solution.py
@@ -53,8 +53,8 @@
     memory_h, norm_h, stab_h, past_k_h, past_v_h, past_i_h, past_f_h, taken_h,
     mixed, key_b, value_b, memory, norm_new, stab_new,
     tok, gain, wg, bias, w_in, w_out, norm, stab, past_k, past_v, past_i, past_f, taken,
-    x_buf, xs, keep, give, near, pair, far, g_own, g_buf,
-    m_low, weights, decay, query_b, outgate_b, from_memory, gated,
+    x_buf, xs, keep, give, near, pair, far, total_c, g_own, g_buf,
+    m_low, weights, decay, spread, carries, query_b, outgate_b, from_memory, gated,
     a_buf, p_buf, q_buf, o_send, o_buf,
     in_sem, w_sem, m_sem, t_send, f_send, x_recv, g_send, g_recv,
     n_send, n_recv, z_send, z_recv, a_send, a_recv, p_send, p_recv, o_ssem, o_rsem,
@@ -80,8 +80,21 @@
     root_core = t0 % 2 == core
     turn = 1 - 2 * (z // max(half // 2, 1))
 
+    upper = z // max(half // 2, 1)
+
+    def flip(p):
+        return p + upper * (half - 1 - 2 * p)
+
     def plane(i):
         return lax.rem(z + i * turn + half, half)
+
+    def order(i):
+        past = (i + flip(z)) // half
+        return flip((half - i) * (1 - past) + (i + flip(z) - half) * past)
+
+    def slot_of(p):
+        below = (flip(p) < flip(z)).astype(jnp.int32)
+        return (half - flip(p)) * (1 - below) + (flip(p) + half - flip(z)) * below
 
     small = [
         pltpu.make_async_copy(tok_h, tok, in_sem.at[0]),
@@ -103,13 +116,13 @@
         ))
     ]
     big = [
-        pltpu.make_async_copy(src, w_in.at[i], w_sem.at[i])
+        pltpu.make_async_copy(src, w_in.at[i], w_sem.at[min(i, 1)])
         for i, src in enumerate((w0_h, w1_h, w2_h, w3_h))
     ]
-    load_out = pltpu.make_async_copy(wo_h, w_out, w_sem.at[4])
+    load_out = pltpu.make_async_copy(wo_h, w_out, w_sem.at[2])
 
     def load(q):
-        return pltpu.make_async_copy(memory_h.at[q], memory.at[q], m_sem.at[q])
+        return pltpu.make_async_copy(memory_h.at[q], memory.at[q], m_sem)
 
     for copy in small + big + late:
         copy.start()
@@ -119,7 +132,22 @@
     barrier = pltpu.get_barrier_semaphore()
     each(n, lambda i: signal(barrier, lax.rem(k + i, n), t), 1)
     each(m, lambda j: signal(barrier, k, lax.rem(t + j, m)), 1)
-    last_at = k % m
+    split = m // 2
+
+    def sum_place(kb):
+        return (kb % 2) * split + (kb // 2) % split
+
+    def sum_block(j):
+        return 2 * (j * split + t % split) + t // split
+
+    last_at = sum_place(k)
+
+    def greet_root(h):
+        @pl.when(jnp.logical_and(h != mine, jnp.logical_not(root)))
+        def _():
+            signal(barrier, t0 * r + h, t0)
+
+    each(r, greet_root)
 
     def greet_last(h):
         kk = t * r + h
@@ -130,49 +158,74 @@
 
     each(r, greet_last)
     both = jnp.logical_and(root, last_at == t).astype(jnp.int32)
-    pl.semaphore_wait(barrier, (n - 1) + (m - 1) + r - both)
+    pl.semaphore_wait(
+        barrier,
+        (n - 1) + (m - 1) + r - both + root.astype(jnp.int32) * (r - 1) * (m - 1),
+    )
 
     small[0].wait()
 
+    def cut(h):
+        return pl.ds(pl.multiple_of(h * width, width), width)
+
     def token_copy(h):
-        cut = pl.ds(pl.multiple_of(h * width, width), width)
-        return remote(tok.at[:, cut], x_buf.at[k], t_send.at[h], x_recv.at[k], t * r + h, t)
-
-    def own_token(h):
-        return jnp.logical_and(root, h == mine)
-
-    def start_token(h):
-        @pl.when(jnp.logical_not(own_token(h)))
-        def _():
-            token_copy(h).start()
-
-    each(r, start_token)
+        return remote(
+            tok.at[:, cut(h)], x_buf.at[k], t_send, x_recv.at[k], t * r + h, t
+        )
+
+    def group_copy(h, tt):
+        return remote(
+            tok.at[:, cut(h)], x_buf.at[k], t_send, x_recv.at[k], t0 * r + h, tt
+        )
+
+    def group_each(act):
+        def at_place(h):
+            def to_tp(j):
+                tt = lax.rem(t + j, m)
+
+                @pl.when(jnp.logical_not(jnp.logical_and(h == mine, j == 0)))
+                def _():
+                    act(group_copy(h, tt))
+
+            each(m, to_tp)
+
+        each(r, at_place)
 
     @pl.when(root)
     def _():
-        x_buf[k] = tok[:, pl.ds(pl.multiple_of(mine * width, width), width)]
+        group_each(lambda copy: copy.start())
+        x_buf[k] = tok[:, cut(mine)]
+
+    @pl.when(jnp.logical_not(root))
+    def _():
+        each(r, lambda h: token_copy(h).start())
 
     def forward(j, i, to):
-        return remote(x_buf.at[j], x_buf.at[j], f_send.at[i, j], x_recv.at[j], k, to)
+        return remote(x_buf.at[j], x_buf.at[j], f_send.at[i], x_recv.at[j], k, to)
 
     def cousin(i):
         return lax.rem(t + 2 * i, m)
 
+    def routed(j, act):
+        outside = j // r != t0
+
+        @pl.when(jnp.logical_and(root, outside))
+        def _():
+            for i in range(1, pairs):
+                act(forward(j, i, cousin(i)))
+
+        @pl.when(jnp.logical_and(root_core, outside))
+        def _():
+            act(forward(j, 0, partner))
+
     def pass_token(j):
         @pl.when(jnp.logical_not(jnp.logical_and(root, j == k)))
         def _():
             remote(
-                tok.at[:, pl.ds(0, width)], x_buf.at[j], t_send.at[0], x_recv.at[j], k, t
+                tok.at[:, pl.ds(0, width)], x_buf.at[j], t_send, x_recv.at[j], k, t
             ).wait_recv()
 
-        @pl.when(root)
-        def _():
-            for i in range(1, pairs):
-                forward(j, i, cousin(i)).start()
-
-        @pl.when(root_core)
-        def _():
-            forward(j, 0, partner).start()
+        routed(j, lambda copy: copy.start())
 
     wg[pl.ds(2 * all_heads, wg.shape[0] - 2 * all_heads), :] = jnp.zeros(
         (wg.shape[0] - 2 * all_heads, local), bf16
@@ -190,50 +243,56 @@
 
     def gate_copy(j):
         return remote(
-            g_own, g_buf.at[j - 1], g_send.at[j - 1], g_recv.at[j - 1], k, lax.rem(t + j, m)
+            g_own, g_buf.at[j - 1], g_send, g_recv, k, lax.rem(t + j, m)
         )
 
     each(m, lambda j: gate_copy(j).start(), 1)
     own_gain = gain[:, pl.ds(pl.multiple_of(k * width, width), width)]
 
-    def scale_plane(p):
-        for side, j in enumerate((p * 2 + x, p * 2 + 1 - x)):
-            xs[p, side * rows : (side + 1) * rows, :] = (
+    def near_copy(c, i):
+        return remote(give.at[c, i], near.at[c, i], n_send, n_recv.at[c, i], beside, t)
+
+    def project(c, start, stop):
+        both = xs[start:stop].reshape((stop - start) * 2 * rows, width)
+        part = jnp.dot(both, w_in[c], preferred_element_type=f32).astype(bf16)
+        for i in range(start, stop):
+            at = (i - start) * 2 * rows
+            give[c, i] = part[at : at + rows]
+            keep[c, i] = part[at + rows : at + 2 * rows]
+
+    def take_plane(p, i):
+        for side, j in enumerate((p * 2 + 1 - x, p * 2 + x)):
+            pass_token(j)
+            xs[i, side * rows : (side + 1) * rows, :] = (
                 x_buf[j].astype(f32) * own_gain
             ).astype(bf16)
 
-    def near_copy(c, p):
-        return remote(
-            give.at[c, p], near.at[c, p], n_send.at[c, p], n_recv.at[c, p], beside, t
-        )
-
-    def project(c, p):
-        part = jnp.dot(xs[p], w_in[c], preferred_element_type=f32)
-        give[c, p] = part[rows:].astype(bf16)
-        near_copy(c, p).start()
-        keep[c, p] = part[:rows].astype(bf16)
-
-    def take_plane(p):
-        pass_token(p * 2 + x)
-        pass_token(p * 2 + 1 - x)
-        scale_plane(p)
-
-    take_plane(z)
-    for c in range(2):
-        big[c].wait()
-        project(c, z)
-    for c in range(2, 4):
-        big[c].wait()
+    take_plane(z, 0)
+    big[0].wait()
+    project(0, 0, 1)
+    near_copy(0, 0).start()
+    pltpu.make_async_copy(w_in.at[pl.ds(1, 3)], w_in.at[pl.ds(1, 3)], w_sem.at[1]).wait()
+    project(1, 0, 1)
+    near_copy(1, 0).start()
 
     def far_plane(i):
         p = plane(i)
-        take_plane(p)
-        for c in range(4):
-            project(c, p)
+        take_plane(p, slot_of(p))
 
     each(half, far_plane, 1)
+    project(0, 1, half)
+    each(half, lambda i: near_copy(0, i).start(), 1)
+    for c in range(1, 4):
+        project(c, 1, half)
+
+    def start_near(i):
+        for c in range(1, 4):
+            near_copy(c, i).start()
+
+    each(half, start_near, 1)
     for c in range(2, 4):
-        project(c, z)
+        project(c, 0, 1)
+        near_copy(c, 0).start()
 
     for copy in late:
         copy.wait()
@@ -257,8 +316,45 @@
         for h in range(heads):
             weights[h, j : j + 1, :] = weight_j[h : h + 1, :]
 
+    remote(g_buf, g_buf, g_send, g_recv, k, t).wait_recv()
+    total = g_own[...]
+    for j in range(m - 1):
+        total = total + g_buf[j]
+    scale = lax.rsqrt(total[:, 2 * all_heads : 2 * all_heads + 1] / features + epsilon)
+    gates = total * scale
+
+    token_row = iota((rows, rows), 0)
+    token_col = iota((rows, rows), 1)
+    same_seq = token_row // chain == token_col // chain
+    causal = jnp.logical_and(same_seq, token_col <= token_row)
+    diagonal = token_row == token_col
+    own_seq = iota((rows, seqs), 0) // chain == iota((rows, seqs), 1)
+    first = t * heads
+
+    def to_row(col):
+        return jnp.sum(jnp.where(diagonal, col, 0.0), axis=0, keepdims=True)
+
+    def pick(array, at):
+        return jnp.sum(
+            jnp.where(iota(array.shape, 1) == at, array, 0.0), axis=1, keepdims=True
+        )
+
+    for h in range(heads):
+        in_col = pick(gates, first + h)
+        forget = pick(gates, all_heads + first + h) + pick(bias[...], first + h)
+        b_col = jnp.sum(
+            jnp.where(causal, to_row(log_sigmoid(forget)), 0.0), axis=1, keepdims=True
+        )
+        within = jnp.where(causal, b_col + to_row(in_col - b_col), -jnp.inf)
+        stab_col = jnp.sum(
+            jnp.where(own_seq, stab_new[h : h + 1, :], 0.0), axis=1, keepdims=True
+        )
+        carried = b_col + stab_col
+        stable = jnp.maximum(carried, jnp.max(within, axis=1, keepdims=True))
+        spread[h] = jnp.exp(within - stable) * key_scale
+        carries[h] = jnp.broadcast_to(jnp.exp(carried - stable), carries.shape[1:])
+
     def take(q):
-        load(q).wait()
         for h in range(heads):
             at = slice(h * dk, (h + 1) * dk)
             w_col = jnp.sum(
@@ -282,45 +378,71 @@
             memory[q, h] = new
             m_low[q, h] = new.astype(bf16)
 
-    def fold(c, p):
-        near_copy(c, p).wait_recv()
-        pair[c, p] = (keep[c, p].astype(f32) + near[c, p].astype(f32)).astype(bf16)
-
-    def far_copy(c, p):
-        slot = lax.rem(z - p + half, half) - 1
+    def line_copy(c, i):
+        p = order(i)
+        left = (p < z).astype(jnp.int32)
+        slot = p + (p == z - 1).astype(jnp.int32) * (half - p)
         return remote(
-            pair.at[c, p], far.at[c, slot], z_send.at[c, p], z_recv.at[c, slot], p * 2 + x, t
-        )
-
-    def fold_plane(i):
-        p = plane(i)
+            pair.at[c, i - 1], far.at[c, slot], z_send, z_recv.at[c, slot],
+            (z + 1 - 2 * left) * 2 + x, t,
+        )
+
+    def line_wait(c, slot):
+        remote(
+            pair.at[c, 0], far.at[c, slot], z_send, z_recv.at[c, slot], k, t
+        ).wait_recv()
+
+    def fold(c, i):
+        p = order(i)
+        near_copy(c, i).wait_recv()
+        starts = jnp.logical_or(
+            jnp.logical_and(p > z, z == 0), jnp.logical_and(p < z, z == half - 1)
+        )
+
+        @pl.when(starts)
+        def _():
+            pair[c, i - 1] = (keep[c, i].astype(f32) + near[c, i].astype(f32)).astype(bf16)
+
+        @pl.when(jnp.logical_not(starts))
+        def _():
+            line_wait(c, p)
+            pair[c, i - 1] = (
+                keep[c, i].astype(f32) + near[c, i].astype(f32) + far[c, p].astype(f32)
+            ).astype(bf16)
+
+        line_copy(c, i).start()
+
+    pltpu.make_async_copy(memory_h, memory, m_sem).wait()
+
+    def fold_query(i):
+        fold(0, i)
         each(seqs * i // (half - 1), take, seqs * (i - 1) // (half - 1))
-        for c in range(4):
-            fold(c, p)
-            far_copy(c, p).start()
-
-    for c in range(2):
-        fold(c, z)
-    each(half, fold_plane, 1)
-
-    def landed_far(c, i):
-        remote(
-            pair.at[c, 0], far.at[c, i], z_send.at[c, 0], z_recv.at[c, i], k, t
-        ).wait_recv()
-
-    each(m, lambda j: gate_copy(j).wait_recv(), 1)
-    total = g_own[...]
-    for j in range(m - 1):
-        total = total + g_buf[j]
-    scale = lax.rsqrt(total[:, 2 * all_heads : 2 * all_heads + 1] / features + epsilon)
-    gates = total * scale
+
+    each(half, fold_query, 1)
+
+    def fold_rest(i):
+        for c in range(1, 4):
+            fold(c, i)
+
+    each(half, fold_rest, 1)
 
     def settle(c, out):
-        each(half - 1, lambda i: landed_far(c, i))
-        summed = pair[c, z].astype(f32)
-        for i in range(half - 1):
-            summed = summed + far[c, i].astype(f32)
-        out[...] = (summed * scale).astype(bf16)
+        near_copy(c, 0).wait_recv()
+        total_c[...] = keep[c, 0].astype(f32) + near[c, 0].astype(f32)
+
+        def add(slot):
+            line_wait(c, slot)
+            total_c[...] += far[c, slot].astype(f32)
+
+        @pl.when(z > 0)
+        def _():
+            add(z)
+
+        @pl.when(z < half - 1)
+        def _():
+            add(half)
+
+        out[...] = (total_c[...] * scale).astype(bf16)
 
     settle(0, query_b)
     row_seq = iota((rows, dv), 0) // chain
@@ -337,85 +459,54 @@
     each(seqs, recall)
     settle(1, key_b)
 
-    token_row = iota((rows, rows), 0)
-    token_col = iota((rows, rows), 1)
-    same_seq = token_row // chain == token_col // chain
-    causal = jnp.logical_and(same_seq, token_col <= token_row)
-    diagonal = token_row == token_col
-    own_seq = iota((rows, seqs), 0) // chain == iota((rows, seqs), 1)
-    first = t * heads
-
-    def to_row(col):
-        return jnp.sum(jnp.where(diagonal, col, 0.0), axis=0, keepdims=True)
-
-    def pick(array, at):
-        return jnp.sum(
-            jnp.where(iota(array.shape, 1) == at, array, 0.0), axis=1, keepdims=True
-        )
-
-    scores, carries, dens = [], [], []
+    scores, dens = [], []
     for h in range(heads):
         at = slice(h * dk, (h + 1) * dk)
-        in_col = pick(gates, first + h)
-        forget = pick(gates, all_heads + first + h) + pick(bias[...], first + h)
-        b_col = jnp.sum(
-            jnp.where(causal, to_row(log_sigmoid(forget)), 0.0), axis=1, keepdims=True
-        )
-        within = jnp.where(causal, b_col + to_row(in_col - b_col), -jnp.inf)
-        stab_col = jnp.sum(
-            jnp.where(own_seq, stab_new[h : h + 1, :], 0.0), axis=1, keepdims=True
-        )
-        carried = b_col + stab_col
-        stable = jnp.maximum(carried, jnp.max(within, axis=1, keepdims=True))
-        carry = jnp.exp(carried - stable)
         match = lax.dot_general(
             query_b[:, at], key_b[:, at], (((1,), (1,)), ((), ())), preferred_element_type=f32
         )
-        score = match * key_scale * jnp.exp(within - stable)
+        score = match * spread[h]
         across_n = lax.dot_general(
             query_b[:, at].astype(f32), norm_new[:, h, :], (((1,), (1,)), ((), ())),
             precision=lax.Precision.HIGHEST, preferred_element_type=f32,
         )
         q_n = jnp.sum(jnp.where(own_seq, across_n, 0.0), axis=1, keepdims=True)
-        den = carry * q_n + jnp.sum(score, axis=1, keepdims=True)
+        den = carries[h, :, :1] * q_n + jnp.sum(score, axis=1, keepdims=True)
         scores.append(score.astype(bf16))
-        carries.append(carry)
         dens.append(1.0 / jnp.maximum(jnp.abs(den), 1.0))
 
-    for c in range(2, 4):
-        fold(c, z)
     settle(2, value_b)
     for h in range(heads):
         at = slice(h * dv, (h + 1) * dv)
         fresh = jnp.dot(scores[h], value_b[:, at], preferred_element_type=f32)
-        from_memory[:, at] = (carries[h] * from_memory[:, at] + fresh) * dens[h]
+        from_memory[:, at] = (carries[h, :, :1] * from_memory[:, at] + fresh) * dens[h]
     settle(3, outgate_b)
     gated[...] = (jax.nn.sigmoid(outgate_b[...].astype(f32)) * from_memory[...]).astype(bf16)
 
     def along_copy(i):
-        return remote(gated, a_buf.at[k], a_send.at[i], a_recv.at[k], plane(i) * 2 + x, t)
+        return remote(gated, a_buf.at[k], a_send, a_recv.at[k], plane(i) * 2 + x, t)
 
     def across_copy(i):
         at = plane(i) * 2 + x
-        return remote(
-            a_buf.at[at], a_buf.at[at], a_send.at[half + i], a_recv.at[at], beside, t
-        )
-
-    own_copy = remote(gated, a_buf.at[k], a_send.at[0], a_recv.at[k], beside, t)
+        return remote(a_buf.at[at], a_buf.at[at], a_send, a_recv.at[at], beside, t)
+
+    own_copy = remote(gated, a_buf.at[k], a_send, a_recv.at[k], beside, t)
     each(half, lambda i: along_copy(i).start(), 1)
     own_copy.start()
     a_buf[k] = gated[...]
     load_out.wait()
 
     def landed(at):
-        remote(gated, a_buf.at[at], a_send.at[0], a_recv.at[at], k, t).wait_recv()
+        remote(gated, a_buf.at[at], a_send, a_recv.at[at], k, t).wait_recv()
 
     def part_copy(kb):
         j = kb // m
-        return remote(p_buf.at[kb], q_buf.at[j, t], p_send.at[kb], p_recv.at[j, t], k, kb % m)
+        return remote(
+            p_buf.at[kb], q_buf.at[j, t], p_send, p_recv.at[j, t], k, sum_place(kb)
+        )
 
     def away(kb):
-        return kb % m != t
+        return sum_place(kb) != t
 
     def mix_plane(p):
         landed(p * 2 + 1 - x)
@@ -438,21 +529,23 @@
     mix_plane(plane(half - 1))
 
     def final_copy(j):
-        return remote(o_send.at[j], o_buf.at[mine], o_ssem.at[j], o_rsem.at[mine], j * m + t, t0)
+        return remote(
+            o_send.at[j], o_buf.at[mine], o_ssem.at[j], o_rsem.at[mine], sum_block(j), t0
+        )
 
     def stays(j):
-        return jnp.logical_and(root, j * m + t == k)
+        return jnp.logical_and(root, sum_block(j) == k)
 
     for j in range(r):
         def landed_part(tt, j=j):
             @pl.when(tt != t)
             def _():
                 remote(
-                    p_buf.at[0], q_buf.at[j, tt], p_send.at[0], p_recv.at[j, tt], k, t
+                    p_buf.at[0], q_buf.at[j, tt], p_send, p_recv.at[j, tt], k, t
                 ).wait_recv()
 
         each(m, landed_part)
-        q_buf[j, t] = p_buf[j * m + t]
+        q_buf[j, t] = p_buf[sum_block(j)]
         summed = q_buf[j, 0].astype(f32)
         for tt in range(1, m):
             summed = summed + q_buf[j, tt].astype(f32)
@@ -475,38 +568,30 @@
 
         mixed[:, h * out_cols : (h + 1) * out_cols] = o_buf[h]
 
-    def drain_token(h):
-        @pl.when(jnp.logical_not(own_token(h)))
-        def _():
-            token_copy(h).wait_send()
-
-    each(r, drain_token)
-
-    def drain_forward(j):
-        @pl.when(root)
-        def _():
-            for i in range(1, pairs):
-                forward(j, i, cousin(i)).wait_send()
-
-        @pl.when(root_core)
-        def _():
-            forward(j, 0, partner).wait_send()
-
-    each(n, drain_forward)
-    each(m, lambda j: gate_copy(j).wait_send(), 1)
-    for c in range(4):
-        each(half, lambda p, c=c: near_copy(c, p).wait_send())
-        each(half, lambda i, c=c: far_copy(c, plane(i)).wait_send(), 1)
-    each(half, lambda i: along_copy(i).wait_send(), 1)
-    own_copy.wait_send()
-    each(half, lambda i: across_copy(i).wait_send(), 1)
-
-    def drain_part(kb):
-        @pl.when(away(kb))
-        def _():
-            part_copy(kb).wait_send()
-
-    each(n, drain_part)
+    @pl.when(root)
+    def _():
+        sent = x_buf.at[pl.ds(0, n - 1)]
+        remote(sent, sent, t_send, x_recv.at[0], k, t).wait_send()
+        for i in range(1, pairs):
+            sent = x_buf.at[pl.ds(0, n - r)]
+            remote(sent, sent, f_send.at[i], x_recv.at[0], k, t).wait_send()
+
+    @pl.when(jnp.logical_not(root))
+    def _():
+        remote(tok, tok, t_send, x_recv.at[0], k, t).wait_send()
+
+    @pl.when(root_core)
+    def _():
+        sent = x_buf.at[pl.ds(0, n - r)]
+        remote(sent, sent, f_send.at[0], x_recv.at[0], k, t).wait_send()
+
+    remote(g_buf, g_buf, g_send, g_recv, k, t).wait_send()
+    remote(give, give, n_send, n_recv.at[0, 0], k, t).wait_send()
+    remote(pair, pair, z_send, z_recv.at[0, 0], k, t).wait_send()
+    sent = a_buf.at[pl.ds(0, n - 1)]
+    remote(sent, sent, a_send, a_recv.at[0], k, t).wait_send()
+    sent = p_buf.at[pl.ds(0, n - r)]
+    remote(sent, sent, p_send, p_recv.at[0, 0], k, t).wait_send()
     for j in range(r):
         @pl.when(jnp.logical_not(stays(j)))
         def _(j=j):
@@ -523,7 +608,6 @@
     depth, out_cols = w_out.shape
     half, r = n // 2, n // m
     lanes = -(-(2 * all_heads + 1) // 128) * 128
-    row_block = jax.ShapeDtypeStruct((rows, cols), bf16)
     V = pltpu.VMEM
     outs = [
         V((rows, local), bf16), V((rows, cols), bf16), V((rows, cols), bf16),
@@ -542,19 +626,19 @@
             V(taken.shape, jnp.int32),
             V((n, rows, width), bf16), V((half, 2 * rows, width), bf16),
             V((4, half, rows, cols), bf16), V((4, half, rows, cols), bf16),
-            V((4, half, rows, cols), bf16), V((4, half, rows, cols), bf16),
-            V((4, half - 1, rows, cols), bf16),
+            V((4, half, rows, cols), bf16), V((4, half - 1, rows, cols), bf16),
+            V((4, half + 1, rows, cols), bf16), V((rows, cols), f32),
             V((rows, lanes), f32), V((m - 1, rows, lanes), f32),
             V(memory.shape, bf16), V((heads, chain, seqs), f32), V(stab.shape, f32),
+            V((heads, rows, rows), f32), V((heads, rows, 128), f32),
             V((rows, cols), bf16), V((rows, cols), bf16), V((rows, cols), f32),
             V((rows, cols), bf16),
             V((n, rows, cols), bf16), V((n, rows, out_cols), bf16),
             V((r, m, rows, out_cols), bf16), V((r, rows, out_cols), bf16),
             V((r, rows, out_cols), bf16),
-            DMA((12,)), DMA((5,)), DMA((seqs,)), DMA((r,)), DMA((m // 2, n)), DMA((n,)),
-            DMA((m - 1,)), DMA((m - 1,)),
-            DMA((4, half)), DMA((4, half)), DMA((4, half)), DMA((4, half - 1)),
-            DMA((n,)), DMA((n,)), DMA((n,)), DMA((r, m)), DMA((r,)), DMA((r,)),
+            DMA((12,)), DMA((3,)), DMA, DMA, DMA((m // 2,)), DMA((n,)), DMA, DMA,
+            DMA, DMA((4, half)), DMA, DMA((4, half + 1)),
+            DMA, DMA((n,)), DMA, DMA((r, m)), DMA((r,)), DMA((r,)),
         ],
         compiler_params=pltpu.CompilerParams(
             collective_id=0, has_side_effects=True, vmem_limit_bytes=40 * 1024 * 1024

time: 68.3 us -> 62.1 us (0.909)
  Pallas kernels: 66.6 us -> 61 us
    pallas_call x1, Pallas kernels: 63.1 us -> 57.5 us  [cell(): pl.pallas_call(functools.partial(cell_kernel, n, m, all_heads, local * m,...]
where the time goes in v2:
time: 62.1 us; the launch traced here: 61.6 us
  Pallas kernels  61 us (98%)
  between operations  0.65 us (1%)
    pallas_call x1, Pallas kernels, cell(): pl.pallas_call(functools.partial(cell_kernel, n, m, all_heads, local * m,...  57.5 us
    pallas_call x1, Pallas kernels, put(): pl.pallas_call(functools.partial(put_kernel, len(arrays), pieces), out_sh...  3.48 us

profile of v2, /device:TPU:5, one launch (start us, length us, event | category | flops | bytes accessed | tf_op | source)
XLA Modules:
  0.0 61.6 jit_solution(6358053532778536546)
XLA Ops:
  0.6 57.5 %shard_map.217 = (bf16[32,1024]{1,0:T(8,128)(2,1)S(1)}, bf16[32,1024]{1,0:T(8,128)(2,1)S(1)}, bf16[32,1024]{1,0:T(8,128)(2,1)S(1)}, f32[8,4,256,256]{3,2,1,0:T(8...) custom-call(bf16[32,1024]{1,0:T(8,128)(2,1)} %tok_h.1, f32[1,4096]{1,0:T(1,128)} %bitcast.11, ...), custom_call_target="tpu_custom_call" | custom-call | tf_op jit(solution)/shard_map/pallas_call | solution.py:616
  58.2 3.5 %shard_map.218 = (bf16[32,1024]{1,0:T(8,128)(2,1)}, bf16[32,1024]{1,0:T(8,128)(2,1)}, bf16[32,1024]{1,0:T(8,128)(2,1)}, f32[8,4,256,256]{3,2,1,0:T(8,128)}, f32[8,4,256]{2,1,0:T(4,128)}, /*index=5*/f32[4,8]{1,0:T(4,128)}) custom-call(bf16[32,1024]{1,0:T(8,128)(2,1)S(1)} %get-tuple-element.18.refs_0_, bf16[32,1024]{1,0:T(8,128)(2,1)S(1)} %get-tuple-element.19.refs_1_, ...), custom_call_target="tpu_custom_call" | custom-call | tf_op jit(solution)/shard_map/pallas_call | solution.py:668

commit v3 on v2

--- a/solution.py
+++ b/solution.py
@@ -78,7 +78,6 @@
     mine = k % r
     root = t0 == t
     root_core = t0 % 2 == core
-    turn = 1 - 2 * (z // max(half // 2, 1))
 
     upper = z // max(half // 2, 1)
 
@@ -86,7 +85,16 @@
         return p + upper * (half - 1 - 2 * p)
 
     def plane(i):
-        return lax.rem(z + i * turn + half, half)
+        at = flip(z)
+        back = jnp.int32(half) - i
+        right = half - 1 - at
+        first = (back < right).astype(jnp.int32)
+        last = (back == half - 1).astype(jnp.int32)
+        return flip(
+            first * (1 - last) * i
+            + (1 - first) * (1 - last) * (back - right)
+            + last * (at + 1)
+        )
 
     def order(i):
         past = (i + flip(z)) // half
@@ -149,6 +157,16 @@
 
     each(r, greet_root)
 
+    @pl.when(jnp.logical_and(root_core, jnp.logical_not(root)))
+    def _():
+        def greet_source(j):
+            @pl.when(j // r != t0)
+            def _():
+                signal(barrier, j, t0)
+
+        each(n, greet_source)
+
+
     def greet_last(h):
         kk = t * r + h
 
@@ -160,17 +178,22 @@
     both = jnp.logical_and(root, last_at == t).astype(jnp.int32)
     pl.semaphore_wait(
         barrier,
-        (n - 1) + (m - 1) + r - both + root.astype(jnp.int32) * (r - 1) * (m - 1),
+        (n - 1) + (m - 1) + r - both
+        + root.astype(jnp.int32) * ((r - 1) * (m - 1) - r * (pairs - 1))
+        + r * (pairs - 1),
     )
 
     small[0].wait()
+
+    def cousin(i):
+        return lax.rem(t + 2 * i, m)
 
     def cut(h):
         return pl.ds(pl.multiple_of(h * width, width), width)
 
-    def token_copy(h):
+    def token_copy(h, i):
         return remote(
-            tok.at[:, cut(h)], x_buf.at[k], t_send, x_recv.at[k], t * r + h, t
+            tok.at[:, cut(h)], x_buf.at[k], t_send, x_recv.at[k], t * r + h, cousin(i)
         )
 
     def group_copy(h, tt):
@@ -198,25 +221,11 @@
 
     @pl.when(jnp.logical_not(root))
     def _():
-        each(r, lambda h: token_copy(h).start())
-
-    def forward(j, i, to):
-        return remote(x_buf.at[j], x_buf.at[j], f_send.at[i], x_recv.at[j], k, to)
-
-    def cousin(i):
-        return lax.rem(t + 2 * i, m)
-
-    def routed(j, act):
-        outside = j // r != t0
-
-        @pl.when(jnp.logical_and(root, outside))
-        def _():
-            for i in range(1, pairs):
-                act(forward(j, i, cousin(i)))
-
-        @pl.when(jnp.logical_and(root_core, outside))
-        def _():
-            act(forward(j, 0, partner))
+        for i in range(pairs):
+            each(r, lambda h, i=i: token_copy(h, i).start())
+
+    def forward(j):
+        return remote(x_buf.at[j], x_buf.at[j], f_send, x_recv.at[j], k, partner)
 
     def pass_token(j):
         @pl.when(jnp.logical_not(jnp.logical_and(root, j == k)))
@@ -225,7 +234,9 @@
                 tok.at[:, pl.ds(0, width)], x_buf.at[j], t_send, x_recv.at[j], k, t
             ).wait_recv()
 
-        routed(j, lambda copy: copy.start())
+        @pl.when(jnp.logical_and(root_core, j // r != t0))
+        def _():
+            forward(j).start()
 
     wg[pl.ds(2 * all_heads, wg.shape[0] - 2 * all_heads), :] = jnp.zeros(
         (wg.shape[0] - 2 * all_heads, local), bf16
@@ -520,12 +531,13 @@
             def _():
                 part_copy(kb).start()
 
-    def step_plane(i):
+    def pass_on(i):
         landed(plane(i) * 2 + x)
         across_copy(i).start()
-        mix_plane(plane(i - 1))
-
-    each(half, step_plane, 1)
+
+    each(half, pass_on, 1)
+    mix_plane(z)
+    each(half - 1, lambda i: mix_plane(plane(i)), 1)
     mix_plane(plane(half - 1))
 
     def final_copy(j):
@@ -572,18 +584,16 @@
     def _():
         sent = x_buf.at[pl.ds(0, n - 1)]
         remote(sent, sent, t_send, x_recv.at[0], k, t).wait_send()
-        for i in range(1, pairs):
-            sent = x_buf.at[pl.ds(0, n - r)]
-            remote(sent, sent, f_send.at[i], x_recv.at[0], k, t).wait_send()
 
     @pl.when(jnp.logical_not(root))
     def _():
-        remote(tok, tok, t_send, x_recv.at[0], k, t).wait_send()
+        sent = x_buf.at[pl.ds(0, r * pairs)]
+        remote(sent, sent, t_send, x_recv.at[0], k, t).wait_send()
 
     @pl.when(root_core)
     def _():
         sent = x_buf.at[pl.ds(0, n - r)]
-        remote(sent, sent, f_send.at[0], x_recv.at[0], k, t).wait_send()
+        remote(sent, sent, f_send, x_recv.at[0], k, t).wait_send()
 
     remote(g_buf, g_buf, g_send, g_recv, k, t).wait_send()
     remote(give, give, n_send, n_recv.at[0, 0], k, t).wait_send()
@@ -636,7 +646,7 @@
             V((n, rows, cols), bf16), V((n, rows, out_cols), bf16),
             V((r, m, rows, out_cols), bf16), V((r, rows, out_cols), bf16),
             V((r, rows, out_cols), bf16),
-            DMA((12,)), DMA((3,)), DMA, DMA, DMA((m // 2,)), DMA((n,)), DMA, DMA,
+            DMA((12,)), DMA((3,)), DMA, DMA, DMA, DMA((n,)), DMA, DMA,
             DMA, DMA((4, half)), DMA, DMA((4, half + 1)),
             DMA, DMA((n,)), DMA, DMA((r, m)), DMA((r,)), DMA((r,)),
         ],

time: 62.1 us -> 61.3 us (0.987)
  no operation moved by 1% of the time
where the time goes in v3:
time: 61.3 us; the launch traced here: 61.1 us
  Pallas kernels  60.5 us (99%)
  between operations  0.65 us (1%)
    pallas_call x1, Pallas kernels, cell(): pl.pallas_call(functools.partial(cell_kernel, n, m, all_heads, local * m,...  57 us
    pallas_call x1, Pallas kernels, put(): pl.pallas_call(functools.partial(put_kernel, len(arrays), pieces), out_sh...  3.48 us

profile of v3, /device:TPU:5, one launch (start us, length us, event | category | flops | bytes accessed | tf_op | source)
XLA Modules:
  0.0 61.1 jit_solution(18339927658055074717)
XLA Ops:
  0.6 57.0 %shard_map.217 = (bf16[32,1024]{1,0:T(8,128)(2,1)S(1)}, bf16[32,1024]{1,0:T(8,128)(2,1)S(1)}, bf16[32,1024]{1,0:T(8,128)(2,1)S(1)}, f32[8,4,256,256]{3,2,1,0:T(8...) custom-call(bf16[32,1024]{1,0:T(8,128)(2,1)} %tok_h.1, f32[1,4096]{1,0:T(1,128)} %bitcast.11, ...), custom_call_target="tpu_custom_call" | custom-call | tf_op jit(solution)/shard_map/pallas_call | solution.py:626
  57.7 3.5 %shard_map.218 = (bf16[32,1024]{1,0:T(8,128)(2,1)}, bf16[32,1024]{1,0:T(8,128)(2,1)}, bf16[32,1024]{1,0:T(8,128)(2,1)}, f32[8,4,256,256]{3,2,1,0:T(8,128)}, f32[8,4,256]{2,1,0:T(4,128)}, /*index=5*/f32[4,8]{1,0:T(4,128)}) custom-call(bf16[32,1024]{1,0:T(8,128)(2,1)S(1)} %get-tuple-element.18.refs_0_, bf16[32,1024]{1,0:T(8,128)(2,1)S(1)} %get-tuple-element.19.refs_1_, ...), custom_call_target="tpu_custom_call" | custom-call | tf_op jit(solution)/shard_map/pallas_call | solution.py:678

commit v4 on v3

--- a/solution.py
+++ b/solution.py
@@ -140,15 +140,11 @@
     barrier = pltpu.get_barrier_semaphore()
     each(n, lambda i: signal(barrier, lax.rem(k + i, n), t), 1)
     each(m, lambda j: signal(barrier, k, lax.rem(t + j, m)), 1)
-    split = m // 2
-
-    def sum_place(kb):
-        return (kb % 2) * split + (kb // 2) % split
-
-    def sum_block(j):
-        return 2 * (j * split + t % split) + t // split
-
-    last_at = sum_place(k)
+    def pair_core(y):
+        return 2 * y + k % 2
+
+    def is_me(kk, tt):
+        return jnp.logical_and(kk == k, tt == t)
 
     def greet_root(h):
         @pl.when(jnp.logical_and(h != mine, jnp.logical_not(root)))
@@ -168,17 +164,16 @@
 
 
     def greet_last(h):
-        kk = t * r + h
-
-        @pl.when(jnp.logical_not(jnp.logical_and(kk == k, last_at == t)))
-        def _():
-            signal(barrier, kk, last_at)
+        for y in range(pairs):
+            @pl.when(jnp.logical_not(is_me(t * r + h, pair_core(y))))
+            def _(y=y):
+                signal(barrier, t * r + h, pair_core(y))
 
     each(r, greet_last)
-    both = jnp.logical_and(root, last_at == t).astype(jnp.int32)
+    both = jnp.logical_and(root, k % 2 == core).astype(jnp.int32)
     pl.semaphore_wait(
         barrier,
-        (n - 1) + (m - 1) + r - both
+        (n - 1) + (m - 1) + half - both
         + root.astype(jnp.int32) * ((r - 1) * (m - 1) - r * (pairs - 1))
         + r * (pairs - 1),
     )
@@ -510,26 +505,41 @@
     def landed(at):
         remote(gated, a_buf.at[at], a_send, a_recv.at[at], k, t).wait_recv()
 
-    def part_copy(kb):
-        j = kb // m
+    def part_copy(p):
         return remote(
-            p_buf.at[kb], q_buf.at[j, t], p_send, p_recv.at[j, t], k, sum_place(kb)
-        )
-
-    def away(kb):
-        return sum_place(kb) != t
+            p_buf.at[p * 2 + 1 - core], q_buf.at[p], p_send, p_recv.at[p], k, partner
+        )
 
     def mix_plane(p):
         landed(p * 2 + 1 - x)
         both_rows = a_buf[pl.ds(p * 2, 2)].reshape(2 * rows, cols)
         part = jnp.dot(both_rows, w_out[...], preferred_element_type=f32).astype(bf16)
         for side in range(2):
-            kb = p * 2 + side
-            p_buf[kb] = part[side * rows : (side + 1) * rows]
-
-            @pl.when(away(kb))
-            def _():
-                part_copy(kb).start()
+            p_buf[p * 2 + side] = part[side * rows : (side + 1) * rows]
+        part_copy(p).start()
+
+    def final_copy(p):
+        return remote(
+            o_send.at[p], o_buf.at[mine, t // 2], o_ssem, o_rsem.at[mine, t // 2],
+            p * 2 + core, t0,
+        )
+
+    def stays(p):
+        return jnp.logical_and(root, p * 2 + core == k)
+
+    def sum_plane(p):
+        part_copy(p).wait_recv()
+        o_send[p] = (
+            p_buf[p * 2 + core].astype(f32) + q_buf[p].astype(f32)
+        ).astype(bf16)
+
+        @pl.when(jnp.logical_not(stays(p)))
+        def _():
+            final_copy(p).start()
+
+        @pl.when(stays(p))
+        def _():
+            o_buf[mine, t // 2] = o_send[p]
 
     def pass_on(i):
         landed(plane(i) * 2 + x)
@@ -537,48 +547,29 @@
 
     each(half, pass_on, 1)
     mix_plane(z)
-    each(half - 1, lambda i: mix_plane(plane(i)), 1)
+
+    def mix_next(i):
+        mix_plane(plane(i))
+        later = (i > 1).astype(jnp.int32)
+        sum_plane(later * plane(i - 1) + (1 - later) * z)
+
+    each(half - 1, mix_next, 1)
     mix_plane(plane(half - 1))
-
-    def final_copy(j):
-        return remote(
-            o_send.at[j], o_buf.at[mine], o_ssem.at[j], o_rsem.at[mine], sum_block(j), t0
-        )
-
-    def stays(j):
-        return jnp.logical_and(root, sum_block(j) == k)
-
-    for j in range(r):
-        def landed_part(tt, j=j):
-            @pl.when(tt != t)
-            def _():
+    if half > 1:
+        sum_plane(plane(half - 2))
+    sum_plane(plane(half - 1))
+    for h in range(r):
+        for y in range(pairs):
+            @pl.when(jnp.logical_not(is_me(t * r + h, pair_core(y))))
+            def _(h=h, y=y):
                 remote(
-                    p_buf.at[0], q_buf.at[j, tt], p_send, p_recv.at[j, tt], k, t
+                    o_send.at[0], o_buf.at[h, y], o_ssem, o_rsem.at[h, y], k, t
                 ).wait_recv()
 
-        each(m, landed_part)
-        q_buf[j, t] = p_buf[sum_block(j)]
-        summed = q_buf[j, 0].astype(f32)
-        for tt in range(1, m):
-            summed = summed + q_buf[j, tt].astype(f32)
-        o_send[j] = summed.astype(bf16)
-
-        @pl.when(jnp.logical_not(stays(j)))
-        def _(j=j):
-            final_copy(j).start()
-
-        @pl.when(stays(j))
-        def _(j=j):
-            o_buf[mine] = o_send[j]
-
-    for h in range(r):
-        @pl.when(jnp.logical_not(jnp.logical_and(t * r + h == k, last_at == t)))
-        def _(h=h):
-            remote(
-                o_send.at[0], o_buf.at[h], o_ssem.at[0], o_rsem.at[h], k, t
-            ).wait_recv()
-
-        mixed[:, h * out_cols : (h + 1) * out_cols] = o_buf[h]
+        summed = o_buf[h, 0].astype(f32)
+        for y in range(1, pairs):
+            summed = summed + o_buf[h, y].astype(f32)
+        mixed[:, h * out_cols : (h + 1) * out_cols] = summed.astype(bf16)
 
     @pl.when(root)
     def _():
@@ -600,12 +591,17 @@
     remote(pair, pair, z_send, z_recv.at[0, 0], k, t).wait_send()
     sent = a_buf.at[pl.ds(0, n - 1)]
     remote(sent, sent, a_send, a_recv.at[0], k, t).wait_send()
-    sent = p_buf.at[pl.ds(0, n - r)]
-    remote(sent, sent, p_send, p_recv.at[0, 0], k, t).wait_send()
-    for j in range(r):
-        @pl.when(jnp.logical_not(stays(j)))
-        def _(j=j):
-            final_copy(j).wait_send()
+    remote(q_buf, q_buf, p_send, p_recv.at[0], k, t).wait_send()
+    keeps = jnp.logical_and(root, k % 2 == core)
+
+    @pl.when(keeps)
+    def _():
+        sent = o_send.at[pl.ds(0, half - 1)]
+        remote(sent, sent, o_ssem, o_rsem.at[0, 0], k, t).wait_send()
+
+    @pl.when(jnp.logical_not(keeps))
+    def _():
+        remote(o_send, o_send, o_ssem, o_rsem.at[0, 0], k, t).wait_send()
 
 
 def cell(n, m, tokens, gain, wi, wf, bias, weights, w_out, memory, norm, stab, past_k, past_v,
@@ -644,11 +640,11 @@
             V((rows, cols), bf16), V((rows, cols), bf16), V((rows, cols), f32),
             V((rows, cols), bf16),
             V((n, rows, cols), bf16), V((n, rows, out_cols), bf16),
-            V((r, m, rows, out_cols), bf16), V((r, rows, out_cols), bf16),
-            V((r, rows, out_cols), bf16),
+            V((half, rows, out_cols), bf16), V((half, rows, out_cols), bf16),
+            V((r, m // 2, rows, out_cols), bf16),
             DMA((12,)), DMA((3,)), DMA, DMA, DMA, DMA((n,)), DMA, DMA,
             DMA, DMA((4, half)), DMA, DMA((4, half + 1)),
-            DMA, DMA((n,)), DMA, DMA((r, m)), DMA((r,)), DMA((r,)),
+            DMA, DMA((n,)), DMA, DMA((half,)), DMA, DMA((r, m // 2)),
         ],
         compiler_params=pltpu.CompilerParams(
             collective_id=0, has_side_effects=True, vmem_limit_bytes=40 * 1024 * 1024

time: 61.3 us -> 58.7 us (0.958)
  Pallas kernels: 60.5 us -> 57.9 us
    pallas_call x1, Pallas kernels: 57 us -> 54.4 us  [cell(): pl.pallas_call(functools.partial(cell_kernel, n, m, all_heads, local * m,...]
where the time goes in v4:
time: 58.7 us; the launch traced here: 58.5 us
  Pallas kernels  57.9 us (99%)
  between operations  0.65 us (1%)
    pallas_call x1, Pallas kernels, cell(): pl.pallas_call(functools.partial(cell_kernel, n, m, all_heads, local * m,...  54.4 us
    pallas_call x1, Pallas kernels, put(): pl.pallas_call(functools.partial(put_kernel, len(arrays), pieces), out_sh...  3.48 us

profile of v4, /device:TPU:5, one launch (start us, length us, event | category | flops | bytes accessed | tf_op | source)
XLA Modules:
  0.0 58.5 jit_solution(7374100203915872637)
XLA Ops:
  0.6 54.4 %shard_map.217 = (bf16[32,1024]{1,0:T(8,128)(2,1)S(1)}, bf16[32,1024]{1,0:T(8,128)(2,1)S(1)}, bf16[32,1024]{1,0:T(8,128)(2,1)S(1)}, f32[8,4,256,256]{3,2,1,0:T(8...) custom-call(bf16[32,1024]{1,0:T(8,128)(2,1)} %tok_h.1, f32[1,4096]{1,0:T(1,128)} %bitcast.11, ...), custom_call_target="tpu_custom_call" | custom-call | tf_op jit(solution)/shard_map/pallas_call | solution.py:622
  55.1 3.5 %shard_map.218 = (bf16[32,1024]{1,0:T(8,128)(2,1)}, bf16[32,1024]{1,0:T(8,128)(2,1)}, bf16[32,1024]{1,0:T(8,128)(2,1)}, f32[8,4,256,256]{3,2,1,0:T(8,128)}, f32[8,4,256]{2,1,0:T(4,128)}, /*index=5*/f32[4,8]{1,0:T(4,128)}) custom-call(bf16[32,1024]{1,0:T(8,128)(2,1)S(1)} %get-tuple-element.18.refs_0_, bf16[32,1024]{1,0:T(8,128)(2,1)S(1)} %get-tuple-element.19.refs_1_, ...), custom_call_target="tpu_custom_call" | custom-call | tf_op jit(solution)/shard_map/pallas_call | solution.py:674

commit v5 on v4

--- a/solution.py
+++ b/solution.py
@@ -545,8 +545,10 @@
         landed(plane(i) * 2 + x)
         across_copy(i).start()
 
-    each(half, pass_on, 1)
+    each(half - 1, pass_on, 1)
     mix_plane(z)
+    if half > 1:
+        pass_on(half - 1)
 
     def mix_next(i):
         mix_plane(plane(i))

time: 58.7 us -> 59 us (level)
  no operation moved by 1% of the time
where the time goes in v5:
time: 59 us; the launch traced here: 58.9 us
  Pallas kernels  58.2 us (99%)
  between operations  0.65 us (1%)
    pallas_call x1, Pallas kernels, cell(): pl.pallas_call(functools.partial(cell_kernel, n, m, all_heads, local * m,...  54.8 us
    pallas_call x1, Pallas kernels, put(): pl.pallas_call(functools.partial(put_kernel, len(arrays), pieces), out_sh...  3.48 us

profile of v5, /device:TPU:5, one launch (start us, length us, event | category | flops | bytes accessed | tf_op | source)
XLA Modules:
  0.0 58.9 jit_solution(5903685349447727283)
XLA Ops:
  0.6 54.8 %shard_map.217 = (bf16[32,1024]{1,0:T(8,128)(2,1)S(1)}, bf16[32,1024]{1,0:T(8,128)(2,1)S(1)}, bf16[32,1024]{1,0:T(8,128)(2,1)S(1)}, f32[8,4,256,256]{3,2,1,0:T(8...) custom-call(bf16[32,1024]{1,0:T(8,128)(2,1)} %tok_h.1, f32[1,4096]{1,0:T(1,128)} %bitcast.11, ...), custom_call_target="tpu_custom_call" | custom-call | tf_op jit(solution)/shard_map/pallas_call | solution.py:624
  55.4 3.5 %shard_map.218 = (bf16[32,1024]{1,0:T(8,128)(2,1)}, bf16[32,1024]{1,0:T(8,128)(2,1)}, bf16[32,1024]{1,0:T(8,128)(2,1)}, f32[8,4,256,256]{3,2,1,0:T(8,128)}, f32[8,4,256]{2,1,0:T(4,128)}, /*index=5*/f32[4,8]{1,0:T(4,128)}) custom-call(bf16[32,1024]{1,0:T(8,128)(2,1)S(1)} %get-tuple-element.18.refs_0_, bf16[32,1024]{1,0:T(8,128)(2,1)S(1)} %get-tuple-element.19.refs_1_, ...), custom_call_target="tpu_custom_call" | custom-call | tf_op jit(solution)/shard_map/pallas_call | solution.py:676
